TPU v7x, 256 devices: a 4x2x16 block of a 4x16x16 slice. The times are simulated.
256 devices in a mesh: grp: 2 (over y), kv: 16 (over z), tp: 8 (over x, core).
Axes of the slice: x: 4, y: 2, z: 16, core: 2. Of those that a mesh axis runs over, the one named last changes fastest.
The devices are a block of a 4x16x16 slice.
Arguments:
- tokens: bfloat16 [128, 4, 4096], P('grp', None, 'kv'), parts along dimension 0, may hold values from -13 to 13, as said below
- norm_gain: bfloat16 [4096], replicated, may hold values from 0.099609375 to 1.8984375
- w_query: bfloat16 [4096, 2048], P('kv', 'tp'), may hold values from -0.09375 to 0.09375
- w_key: bfloat16 [4096, 2048], P('kv', 'tp'), may hold values from -0.09375 to 0.09375
- w_value: bfloat16 [4096, 2048], P('kv', 'tp'), may hold values from -0.09375 to 0.09375
- w_outgate: bfloat16 [4096, 2048], P('kv', 'tp'), may hold values from -0.09375 to 0.09375
- gate_weight: bfloat16 [2, 4096, 16], replicated, may hold values from -0.09375 to 0.09375
- input_bias: float32 [16], P('tp'), may hold values from -1 to 1
- forget_bias: float32 [16], P('tp'), may hold values from -1 to 4
- w_out: bfloat16 [2048, 4096], P('tp', 'kv'), may hold values from -0.125 to 0.125
- saved_memory: float32 [128, 5, 16, 128, 128], P(('grp', 'kv'), None, 'tp'), parts along dimension 0, may hold values from -0.6 to 0.6
- saved_normalizer: float32 [128, 5, 16, 128], P(('grp', 'kv'), None, 'tp'), parts along dimension 0, may hold values from -0.6 to 0.6
- saved_stabilizer: float32 [128, 5, 16], P(('grp', 'kv'), None, 'tp'), parts along dimension 0, may hold values from -1 to 2
- accepted: int32 [128], P(('grp', 'kv')), parts along dimension 0, may hold values from 0 to 4
Outputs:
- mixed: bfloat16 [128, 4, 4096], P('grp', None, ('kv', 'tp')), parts along dimension 0
- new_memory: float32 [128, 5, 16, 128, 128], P(('grp', 'kv'), None, 'tp'), parts along dimension 0
- new_normalizer: float32 [128, 5, 16, 128], P(('grp', 'kv'), None, 'tp'), parts along dimension 0
- new_stabilizer: float32 [128, 5, 16], P(('grp', 'kv'), None, 'tp'), parts along dimension 0
There are 2 independent parts, one for each index of `grp`. A program takes and returns all parts, laid end to end along the dimension named above; an argument that names none is the same for every part. Nothing has to cross between parts.
Inputs may be any that keep to these rules, and one draw needn't show every extreme that they name: `tokens`: the proposals' activations.
All inputs are finite; a program needn't handle non-finite values.
Results may differ from a plain program's by a relative error of at most 0.015.
The roundings to bfloat16 on the way count: a program that leaves them out, or rounds other values in their place, can miss the bound.
Values may be sent and summed in bfloat16 or wider, within the bound.
No kernel may reach another device: no remote copies, remote signals or barrier semaphores. Data moves between devices by JAX's collectives and lax.ppermute only.
A program may use at most 64 MiB of HBM per device.

v0:
```python
import math

import jax
import jax.numpy as jnp
from jax import lax
from jax.sharding import PartitionSpec as P

D = 4096


EPSILON = 1e-06


def cut_along(value, dim, size):
    before, after = (value.shape[:dim], value.shape[dim + 1 :])
    return jnp.moveaxis(value.reshape(*before, size, -1, *after), dim, 0)


def summed_on_arrival(value, axis, dim):
    parts = cut_along(value, dim, lax.axis_size(axis))
    arrived = lax.all_to_all(parts, axis, split_axis=0, concat_axis=0, tiled=True)
    return arrived.sum(axis=0)


def sent_together(arrays, axis, dim, along):
    widths = [math.prod(a.shape[along:]) for a in arrays]
    both = jnp.concatenate(
        [a.reshape(*a.shape[:along], w) for a, w in zip(arrays, widths)], axis=along
    )
    out = summed_on_arrival(both, axis, dim)
    parts = jnp.split(out, [sum(widths[:k]) for k in range(1, len(widths))], axis=along)
    return tuple((b.reshape(*out.shape[:along], *a.shape[along:]) for a, b in zip(arrays, parts)))


def from_everyone(value, axis):
    size = lax.axis_size(axis)
    return lax.all_to_all(
        jnp.broadcast_to(value[None], (size, *value.shape)), axis, 0, 0, tiled=True
    )


def in_order(parts, dim):
    parts = jnp.moveaxis(parts, 0, dim)
    dims = parts.shape
    return parts.reshape(*dims[:dim], dims[dim] * dims[dim + 1], *dims[dim + 2 :])


def gathered_copies(value, axis, dim):
    parts = from_everyone(value, axis)
    return in_order(parts, dim)


def sent_and_summed(value, axis, dim):
    parts = cut_along(value, dim, lax.axis_size(axis))
    arrived = lax.all_to_all(parts, axis, split_axis=0, concat_axis=0, tiled=True)
    return arrived.astype(jnp.float32).sum(axis=0)


def advance(queries, key_rows, value_rows, in_gate, log_forget, memory, normalizer, stabilizer):
    key_scale = key_rows.shape[-1] ** (-0.5)
    outputs = []
    memories, normalizers, stabilizers = ([memory], [normalizer], [stabilizer])
    for position in range(queries.shape[1]):
        query_now = queries[:, position].astype(jnp.float32)
        key_now = key_rows[:, position].astype(jnp.float32) * key_scale
        value_now = value_rows[:, position].astype(jnp.float32)
        carried = log_forget[:, position] + stabilizer
        incoming = in_gate[:, position]
        top_value = jnp.maximum(carried, incoming)
        retain = jnp.exp(carried - top_value)
        admit_weight = jnp.exp(incoming - top_value)
        memory = retain[..., None, None] * memory + admit_weight[..., None, None] * (
            key_now[..., :, None] * value_now[..., None, :]
        )
        normalizer = retain[..., None] * normalizer + admit_weight[..., None] * key_now
        stabilizer = top_value
        numerator = jnp.einsum("bhd,bhdv->bhv", query_now, memory)
        denominator = jnp.sum(query_now * normalizer, -1)
        floor_value = jnp.exp(-stabilizer)
        outputs.append(numerator / jnp.maximum(jnp.abs(denominator), floor_value)[..., None])
        memories.append(memory)
        normalizers.append(normalizer)
        stabilizers.append(stabilizer)
    return (
        jnp.stack(outputs, 1),
        jnp.stack(memories, 1),
        jnp.stack(normalizers, 1),
        jnp.stack(stabilizers, 1),
    )


def local(
    tokens,
    norm_gain,
    w_query,
    w_key,
    w_value,
    w_outgate,
    gate_weight,
    input_bias,
    forget_bias,
    w_out,
    saved_memory,
    saved_normalizer,
    saved_stabilizer,
    accepted,
):
    local_heads = input_bias.shape[0]
    proposals = tokens.shape[1]
    local_gates = lax.dynamic_slice_in_dim(
        gate_weight, lax.axis_index("tp") * local_heads, local_heads, 2
    )
    slice_width = tokens.shape[2]
    seq_total = tokens.shape[0]
    row_start = lax.axis_index("kv") * slice_width
    floats = tokens.astype(jnp.float32)
    squares = jnp.sum(floats * floats, -1)
    gain_part = lax.dynamic_slice_in_dim(norm_gain, row_start, slice_width, 0)
    scaled = (floats * gain_part.astype(jnp.float32)).astype(jnp.bfloat16).reshape(-1, slice_width)
    row_gates = lax.dynamic_slice_in_dim(local_gates, row_start, slice_width, 1)

    def local_term(weight):
        return jnp.dot(scaled, weight, preferred_element_type=jnp.float32).reshape(
            seq_total, proposals, -1
        )

    reduced = sent_together(
        (
            local_term(w_query),
            local_term(w_key),
            local_term(w_value),
            local_term(w_outgate),
            local_term(row_gates[0]),
            local_term(row_gates[1]),
            squares,
        ),
        "kv",
        0,
        2,
    )
    own_seqs = reduced[0].shape[0]
    inverse = lax.rsqrt(reduced[6] / D + EPSILON).reshape(-1, 1)
    sums = tuple((item.reshape(own_seqs * proposals, -1) for item in reduced[:4]))
    gate_in = reduced[4].reshape(own_seqs * proposals, -1)
    gate_forget = reduced[5].reshape(own_seqs * proposals, -1)

    def finish(summed):
        return (summed * inverse).astype(jnp.bfloat16).reshape(own_seqs, proposals, local_heads, -1)

    queries = finish(sums[0])
    key_rows = finish(sums[1])
    value_rows = finish(sums[2])
    out_gate = finish(sums[3])
    in_gate = (gate_in * inverse).reshape(own_seqs, proposals, local_heads) + input_bias
    log_forget = jax.nn.log_sigmoid(
        (gate_forget * inverse).reshape(own_seqs, proposals, local_heads) + forget_bias
    )
    memory = jnp.take_along_axis(saved_memory, accepted[:, None, None, None, None], 1)[:, 0]
    normalizer = jnp.take_along_axis(saved_normalizer, accepted[:, None, None, None], 1)[:, 0]
    stabilizer = jnp.take_along_axis(saved_stabilizer, accepted[:, None, None], 1)[:, 0]
    hidden, new_memory, new_normalizer, new_stabilizer = advance(
        queries, key_rows, value_rows, in_gate, log_forget, memory, normalizer, stabilizer
    )
    gated = (jax.nn.sigmoid(out_gate.astype(jnp.float32)) * hidden).astype(jnp.bfloat16)
    gated = gated.reshape(own_seqs, proposals, -1)
    piece = gathered_copies(gated, "kv", 0)
    rows = jnp.dot(piece.reshape(-1, piece.shape[-1]), w_out, preferred_element_type=jnp.float32)
    terms = rows.reshape(piece.shape[0], proposals, -1)
    mixed = sent_and_summed(terms.astype(jnp.bfloat16), "tp", 2).astype(jnp.bfloat16)
    return (mixed, new_memory, new_normalizer, new_stabilizer)


def solution(mesh):
    return jax.shard_map(
        local,
        mesh=mesh,
        in_specs=(
            P("grp", None, "kv"),
            P(),
            P("kv", "tp"),
            P("kv", "tp"),
            P("kv", "tp"),
            P("kv", "tp"),
            P(),
            P("tp"),
            P("tp"),
            P("tp", "kv"),
            P(("grp", "kv"), None, "tp", None, None),
            P(("grp", "kv"), None, "tp", None),
            P(("grp", "kv"), None, "tp"),
            P(("grp", "kv")),
        ),
        out_specs=(
            P("grp", None, ("kv", "tp")),
            P(("grp", "kv"), None, "tp", None, None),
            P(("grp", "kv"), None, "tp", None),
            P(("grp", "kv"), None, "tp"),
        ),
        check_vma=False,
    )
```

profile of v0, /device:TPU:33, one launch (start us, length us, event | category | flops | bytes accessed | tf_op | source)
XLA Modules:
  0.0 148.1 jit_solution(547370374483931141)
XLA Ops:
  0.7 0.9 dynamic-slice_convert_fusion
  1.6 1.1 fusion.11
  2.6 1.0 fusion.47
  3.7 1.0 fusion.45
  4.7 0.5 copy.226
  5.2 0.2 copy.224
  5.4 0.8 copy.225
  6.2 1.1 fusion.41
  7.4 1.1 fusion.39
  8.5 0.8 concatenate.18
  9.2 1.0 copy.222
  10.2 1.8 %fusion.37 = f32[64,4,256]{2,0,1:T(8,128)} fusion(bf16[256,256]{1,0:T(8,128)(2,1)} %param.19, bf16[64,4,256]{2,1,0:T(4,128)(2,1)S(1)} %get-tuple-element.49), kind=kOutput, calls=%fused_computation.51 | convolution fusion | flops 33554432 | bytes 524288 | tf_op jit(solution)/shard_map/dot_general | solution.py:123
  12.0 1.7 %concatenate.19 = f32[16,4,4,256]{3,1,0,2:T(4,128)} reshape(f32[64,4,256]{2,0,1:T(8,128)} %fusion.37) | data formatting | bytes 524288 | tf_op jit(solution)/shard_map/concatenate | solution.py:27
  13.7 1.7 %copy.223 = f32[16,4,4,256]{3,1,2,0:T(4,128)} copy(f32[16,4,4,256]{3,1,0,2:T(4,128)} %concatenate.19) | data formatting | bytes 524288 | tf_op jit(solution)/shard_map/concatenate | solution.py:27
  15.4 1.8 %fusion.43 = f32[64,4,256]{2,0,1:T(8,128)} fusion(bf16[256,256]{1,0:T(8,128)(2,1)} %param.16, bf16[64,4,256]{2,1,0:T(4,128)(2,1)S(1)} %get-tuple-element.49), kind=kOutput, calls=%fused_computation.57 | convolution fusion | flops 33554432 | bytes 524288 | tf_op jit(solution)/shard_map/dot_general | solution.py:123
  17.2 1.7 %concatenate.16 = f32[16,4,4,256]{3,1,0,2:T(4,128)} reshape(f32[64,4,256]{2,0,1:T(8,128)} %fusion.43) | data formatting | bytes 524288 | tf_op jit(solution)/shard_map/concatenate | solution.py:27
  18.9 1.7 %copy.220 = f32[16,4,4,256]{3,1,2,0:T(4,128)} copy(f32[16,4,4,256]{3,1,0,2:T(4,128)} %concatenate.16) | data formatting | bytes 524288 | tf_op jit(solution)/shard_map/concatenate | solution.py:27
  20.6 3.3 %concatenate.21 = f32[16,4,4,1029]{3,1,2,0:T(4,128)} concatenate(f32[16,4,4,256]{3,1,2,0:T(4,128)} %copy.220, f32[16,4,4,256]{3,1,2,0:T(4,128)S(1)} %copy.221, f32[16,4,4,256]{3,1,2,0:T(4,128)S(1)} %copy.222, f32[16,4,4,256]{3,1,2,0:T(4,128)} %copy.223, f32[16,4,4,2]{3,1,2,0:T(4,128)S(1)} %copy.224, f32[16,4,4,2]{3,1,2,0:T(4,128)} %copy.225, f32[16,4,4,1]{3,1,2,0:T(4,128)S(1)} %copy.226), dimensions={3} | concatenate | bytes 2107392 | tf_op jit(solution)/shard_map/concatenate | solution.py:27
  24.0 24.6 %all-to-all-start = ((f32[16,4,4,1029]{3,1,2,0:T(4,128)}), f32[16,4,4,1029]{3,1,2,0:T(4,128)}, u32[]{:S(2)}, u32[]{:S(2)}) async-start(f32[16,4,4,1029]{3,1,2,0:T(4,128)} %concatenate.21), calls=%async_computation | async-start | bytes 2359296 | tf_op jit(solution)/shard_map/all_to_all | solution.py:21
  48.6 0.1 copy.233
  48.8 1.3 gather_fusion.2
  50.1 0.6 gather_fusion
  50.7 0.6 gather_fusion.1
  51.4 0.9 fusion.5
  52.3 47.0 %all-to-all-done = f32[16,4,4,1029]{3,1,2,0:T(4,128)} async-done(((f32[16,4,4,1029]{3,1,2,0:T(4,128)}), f32[16,4,4,1029]{3,1,2,0:T(4,128)}, u32[]{:S(2)}, u32[]{:S(2)}) %all-to-all-start) | async-done | bytes 1053728 | tf_op jit(solution)/shard_map/all_to_all | solution.py:21
  99.3 1.5 reduce_sum.67
  100.8 0.1 copy.289
  100.9 0.1 copy.229
  101.0 0.1 fusion.55
  101.2 0.1 copy.250
  101.3 0.1 copy.251
  101.4 0.1 copy.245
  101.5 0.1 copy.246
  101.6 0.1 copy.240
  101.7 0.1 copy.241
  101.9 0.1 copy.236
  102.0 0.1 copy.269
  102.1 0.1 copy.268
  102.2 0.1 copy.267
  102.3 0.1 copy.266
  102.4 0.1 copy.265
  102.5 0.1 stack.43
  102.6 0.6 copy.270
  103.5 0.1 multiply_convert_fusion.2
  103.8 0.1 constant_dynamic-update-slice_fusion.3
  103.9 0.2 multiply_reduce_fusion
  104.1 0.3 fusion.80
  104.4 0.5 fusion.6
  105.0 0.6 fusion.9
  105.7 1.0 fusion
  107.0 0.7 broadcast_in_dim.37
  107.7 13.1 %all-to-all-start.1 = ((bf16[16,4,4,256]{3,1,2,0:T(4,128)(2,1)}), bf16[16,4,4,256]{3,1,2,0:T(4,128)(2,1)S(1)}, u32[]{:S(2)}, u32[]{:S(2)}) async-start(bf16[16,4,4,256]{3,1,2,0:T(4,128)(2,1)} %broadcast_in_dim.37), calls=%async_computation.1 | async-start | bytes 262144 | tf_op jit(solution)/shard_map/all_to_all | solution.py:37
  120.8 1.0 constant_dynamic-update-slice_fusion
  121.9 1.2 fusion.7
  123.1 1.4 fusion.8
  124.5 1.5 %add_dynamic-update-slice_fusion = f32[4,5,2,128,128]{4,3,2,1,0:T(8,128)} fusion(f32[4,5,2,128,128]{4,3,2,1,0:T(8,128)} %fusion.8, f32[4,2,128]{2,1,0:T(2,128)S(1)} %get-tuple-element.72, f32[4,2,128]{2,1,0:T(2,128)S(1)} %get-tuple-element.67, f32[4,2]{1,0:T(4,128)S(1)} %get-tuple-element.36, f32[4,2]{1,0:T(4,128)S(1)} %get-tuple-element.58, ...), kind=kLoop, calls=%fused_computation.5 | loop fusion | flops 2228224 | bytes 1081604 | tf_op jit(solution)/shard_map/stack | solution.py:86
  126.0 6.6 %all-to-all-done.1 = bf16[16,4,4,256]{3,1,2,0:T(4,128)(2,1)S(1)} async-done(((bf16[16,4,4,256]{3,1,2,0:T(4,128)(2,1)}), bf16[16,4,4,256]{3,1,2,0:T(4,128)(2,1)S(1)}, u32[]{:S(2)}, u32[]{:S(2)}) %all-to-all-start.1) | async-done | bytes 131104 | tf_op jit(solution)/shard_map/all_to_all | solution.py:37
  132.7 0.2 convolution_convert_fusion
  132.9 0.2 copy.256
  133.1 0.9 reshape.1113
  134.0 7.9 %all-to-all-start.2 = ((bf16[8,2,4096]{2,1,0:T(2,128)(2,1)}), bf16[8,2,4096]{2,1,0:T(2,128)(2,1)S(1)}, u32[]{:S(2)}, u32[]{:S(2)}) async-start(bf16[8,2,4096]{2,1,0:T(2,128)(2,1)} %reshape.1113), calls=%async_computation.2 | async-start | bytes 262144 | tf_op jit(solution)/shard_map/all_to_all | solution.py:55
  142.0 5.1 %all-to-all-done.2 = bf16[8,2,4096]{2,1,0:T(2,128)(2,1)S(1)} async-done(((bf16[8,2,4096]{2,1,0:T(2,128)(2,1)}), bf16[8,2,4096]{2,1,0:T(2,128)(2,1)S(1)}, u32[]{:S(2)}, u32[]{:S(2)}) %all-to-all-start.2) | async-done | bytes 131104 | tf_op jit(solution)/shard_map/all_to_all | solution.py:55
  147.2 0.2 reshape.1114
  147.4 0.7 bitcast_reduce_fusion
  (49 shorter events, 1.6 us)
Async XLA Ops:
  0.6 50.0 %copy-start = (f32[4,5,2,128,128]{4,3,2,1,0:T(8,128)S(1)}, f32[4,5,2,128,128]{4,3,2,1,0:T(8,128)}, u32[]{:S(2)}) copy-start(f32[4,5,2,128,128]{4,3,2,1,0:T(8,128)} %param.24) | copy-start | bytes 7864324
  18.9 29.7 %copy-start.2 = (f32[4,5,2]{1,2,0:T(2,128)S(1)}, f32[4,5,2]{1,2,0:T(2,128)}, u32[]{:S(2)}) copy-start(f32[4,5,2]{1,2,0:T(2,128)} %param.26) | copy-start | bytes 484
  20.6 28.1 %copy-start.6 = (s32[4]{0:T(128)S(1)}, s32[4]{0:T(128)}, u32[]{:S(2)}) copy-start(s32[4]{0:T(128)} %param.27) | copy-start | bytes 52
  24.0 77.0 %copy-start.4 = (f32[2]{0:T(128)S(1)}, f32[2]{0:T(128)}, u32[]{:S(2)}) copy-start(f32[2]{0:T(128)} %param.22) | copy-start | bytes 28
  24.0 77.0 %copy-start.5 = (f32[2]{0:T(128)S(1)}, f32[2]{0:T(128)}, u32[]{:S(2)}) copy-start(f32[2]{0:T(128)} %param.21) | copy-start | bytes 28
  24.0 75.3 %all-to-all-start = ((f32[16,4,4,1029]{3,1,2,0:T(4,128)}), f32[16,4,4,1029]{3,1,2,0:T(4,128)}, u32[]{:S(2)}, u32[]{:S(2)}) async-start(f32[16,4,4,1029]{3,1,2,0:T(4,128)} %concatenate.21), calls=%async_computation | async-start | bytes 2359296 | tf_op jit(solution)/shard_map/all_to_all | solution.py:21
  107.0 25.7 %copy-start.1 = (bf16[256,256]{1,0:T(8,128)(2,1)S(1)}, bf16[256,256]{1,0:T(8,128)(2,1)}, u32[]{:S(2)}) copy-start(bf16[256,256]{1,0:T(8,128)(2,1)} %param.23) | copy-start | bytes 393220
  107.7 24.9 %all-to-all-start.1 = ((bf16[16,4,4,256]{3,1,2,0:T(4,128)(2,1)}), bf16[16,4,4,256]{3,1,2,0:T(4,128)(2,1)S(1)}, u32[]{:S(2)}, u32[]{:S(2)}) async-start(bf16[16,4,4,256]{3,1,2,0:T(4,128)(2,1)} %broadcast_in_dim.37), calls=%async_computation.1 | async-start | bytes 262144 | tf_op jit(solution)/shard_map/all_to_all | solution.py:37
  134.0 13.2 %all-to-all-start.2 = ((bf16[8,2,4096]{2,1,0:T(2,128)(2,1)}), bf16[8,2,4096]{2,1,0:T(2,128)(2,1)S(1)}, u32[]{:S(2)}, u32[]{:S(2)}) async-start(bf16[8,2,4096]{2,1,0:T(2,128)(2,1)} %reshape.1113), calls=%async_computation.2 | async-start | bytes 262144 | tf_op jit(solution)/shard_map/all_to_all | solution.py:55
  142.0 6.0 %copy-start.3 = (f32[4,5,2,128]{3,2,1,0:T(2,128)}, f32[4,5,2,128]{3,2,1,0:T(2,128)S(1)}, u32[]{:S(2)}) copy-start(f32[4,5,2,128]{3,2,1,0:T(2,128)S(1)} %constant_dynamic-update-slice_fusion.1) | copy-start | bytes 61444
where the time goes:
time: 149 us; the launch traced here: 148 us
  waiting for transfers between devices  58.8 us (39%)
  starting transfers between devices  45.7 us (31%)
  local copies, waits for them, and re-layouts  20.5 us (14%)
  other arithmetic  11.7 us (8%)
  matrix products  10.4 us (7%)
    all_to_all x1, waiting for transfers between devices, summed_on_arrival(): lax.all_to_all(parts, axis, split_axis=0, concat_axis=0, tiled=True)  47 us
    all_to_all x1, starting transfers between devices, summed_on_arrival(): lax.all_to_all(parts, axis, split_axis=0, concat_axis=0, tiled=True)  24.6 us
    all_to_all x1, starting transfers between devices, from_everyone(): lax.all_to_all(jnp.broadcast_to(value[None], (size, *value.shape)), axis,...  13.1 us
    concatenate x10, local copies, waits for them, and re-layouts, sent_together(): jnp.concatenate([a.reshape(*a.shape[:along], w) for a, w in zip(arrays, w...  12.5 us
    all_to_all x1, starting transfers between devices, sent_and_summed(): lax.all_to_all(parts, axis, split_axis=0, concat_axis=0, tiled=True)  7.92 us
    dot_general x6, matrix products, local_term(): jnp.dot(scaled, weight, preferred_element_type=jnp.float32)  7.78 us
    all_to_all x1, waiting for transfers between devices, from_everyone(): lax.all_to_all(jnp.broadcast_to(value[None], (size, *value.shape)), axis,...  6.63 us
    all_to_all x1, waiting for transfers between devices, sent_and_summed(): lax.all_to_all(parts, axis, split_axis=0, concat_axis=0, tiled=True)  5.14 us
  transfers between devices with their start and end apart: 3, of which 3 were waited for; matrix products, arithmetic and copies ran while one was open for 6% of the time, Pallas kernels for 0%

commit v1 on v0

v1 whole, which is shorter than its diff:
```python
import functools

import jax
import jax.numpy as jnp
from jax import lax
from jax.experimental import pallas as pl
from jax.experimental.pallas import tpu as pltpu
from jax.sharding import PartitionSpec as P

EPSILON = 1e-06
F32 = jnp.float32
BF16 = jnp.bfloat16


def iota(shape, dim):
    return lax.broadcasted_iota(jnp.int32, shape, dim)


def contract(a, b, da, db):
    return lax.dot_general(a, b, (((da,), (db,)), ((), ())), preferred_element_type=F32)


def project_kernel(place, tokens, gain, gates, wq, wk, wv, wo, out, *, owners):
    z, tp = place[0], place[1]
    seqs, props, width = tokens.shape
    rows = seqs * props
    per = rows // owners
    own = per // props
    x = tokens[...].astype(F32).reshape(rows, width)
    gain_rows = gain[...].astype(F32)
    pieces = []
    for j in range(width // 128):
        hit = iota(gain_rows.shape, 0) == z * (width // 128) + j
        pieces.append(jnp.sum(jnp.where(hit, gain_rows, 0.0), 0, keepdims=True))
    scaled = (x * jnp.concatenate(pieces, 1)).astype(BF16)
    r, c = iota((rows, rows), 0), iota((rows, rows), 1)
    source = (r // per) * per + (r % own) * props + (r % per) // own
    move = jnp.where(c == source, 1.0, 0.0).astype(BF16)
    scaled = contract(move, scaled, 1, 0).astype(BF16)
    block = 0
    for w in (wq, wk, wv, wo):
        y = contract(scaled, w[...], 1, 0).astype(BF16)
        for h in range(y.shape[1] // 128):
            out[:, block * per : (block + 1) * per, :] = y[:, h * 128 : (h + 1) * 128].reshape(owners, per, 128)
            block += 1
    heads = gates.shape[1]
    local = 2
    pick_r, pick_c = iota((8, 2 * heads), 0), iota((8, 2 * heads), 1)
    want = ((pick_r % 4) // local) * heads + tp * local + pick_r % local
    pick = jnp.where(pick_c == want, 1.0, 0.0).astype(BF16)
    own_gates = contract(pick, gates[...].reshape(2 * heads, width), 1, 0).astype(BF16)
    g = contract(own_gates, scaled, 1, 1)
    square = x * x
    s_hi = square.astype(BF16)
    s_lo = (square - s_hi.astype(F32)).astype(BF16)
    ones = jnp.ones((8, width), BF16)
    s = contract(ones, contract(move, s_hi, 1, 0).astype(BF16), 1, 1)
    s += contract(ones, contract(move, s_lo, 1, 0).astype(BF16), 1, 1)

    def words(value, split):
        hi = value.astype(BF16).astype(F32)
        return jnp.where(iota(value.shape, 0) < split, hi, value - hi)

    g, s = words(g, 4), words(s, 1)
    lanes = iota((8, 128), 1)
    span = 128 // per
    for half in range(rows // 128):
        gh = g[:, half * 128 : (half + 1) * 128]
        sh = pltpu.roll(s[:, half * 128 : (half + 1) * 128], 64, 1)
        low = jnp.where(lanes < 64, gh, sh).astype(BF16)
        high = jnp.where(lanes < 64, sh, gh).astype(BF16)
        for k in range(span):
            out[half * span + k, block * per :, :] = low if k < span // 2 else high


def cell_kernel(place, accepted, stab, ib, fb, got, m0, n0, gated, kv_out, coef, new_n, new_s, *, features):
    z = place[0]
    owners = got.shape[0]
    own, _, heads, dim, _ = m0.shape
    total = got[0].astype(F32)
    for k in range(1, owners):
        total = total + got[k].astype(F32)
    per = (total.shape[0] - 8) // (4 * heads)
    props = per // own
    small = total[4 * heads * per :]
    shift = (z % (128 // per)) * per
    small = pltpu.roll(small, lax.rem(128 - shift, 128), 1)
    g = small + pltpu.roll(small, 4, 0)
    sq = pltpu.roll(small + pltpu.roll(small, 7, 0), 64, 1)
    packed = jnp.where(iota(g.shape, 0) < 4, g, pltpu.roll(sq, 4, 0))
    cols = packed.T[:per]
    inverse = lax.rsqrt(cols[:, 4:5] / features + EPSILON)
    col = iota((per, heads), 1)
    ibv = jnp.where(col == 0, ib[0], ib[1])
    fbv = jnp.where(col == 0, fb[0], fb[1])
    in_gate = cols[:, 0:2] * inverse + ibv
    f = cols[:, 2:4] * inverse + fbv
    log_forget = jnp.minimum(f, 0.0) - jnp.log1p(jnp.exp(-jnp.abs(f)))
    srow, scol = iota((own, heads), 0), iota((own, heads), 1)
    m = jnp.zeros((own, heads), F32)
    for b in range(own):
        for h in range(heads):
            m = jnp.where((srow == b) & (scol == h), stab[b, h, accepted[b]], m)
    stabs, retain, admit = [m], [], []
    for t in range(props):
        carried = log_forget[t * own : (t + 1) * own] + m
        incoming = in_gate[t * own : (t + 1) * own]
        top = jnp.maximum(carried, incoming)
        retain.append(jnp.exp(carried - top))
        admit.append(jnp.exp(incoming - top))
        m = top
        stabs.append(m)
    scale = dim ** (-0.5)
    rr = iota((per, dim), 0) % own
    outs = []
    for h in range(heads):

        def part(kind):
            at = (kind * heads + h) * per
            return (total[at : at + per] * inverse).astype(BF16)

        q, k, v, o = part(0), part(1), part(2), part(3)
        kv_out[h] = k
        kv_out[heads + h] = v
        qf, kf, vf = q.astype(F32), k.astype(F32) * scale, v.astype(F32)
        base = jnp.zeros((per, dim), F32)
        for b in range(own):
            mine = jnp.where(rr == b, qf, 0.0).astype(BF16)
            mem = m0[b, 0, h]
            hi = mem.astype(BF16)
            lo = (mem - hi.astype(F32)).astype(BF16)
            base += contract(mine, hi, 1, 0) + contract(mine, lo, 1, 0)
        norm = n0[:, h, :]
        new_n[:, 0, h, :] = norm
        rows = []
        for t in range(props):
            sl = slice(t * own, (t + 1) * own)
            rt, at = retain[t][:, h : h + 1], admit[t][:, h : h + 1]
            norm = rt * norm + at * kf[sl]
            new_n[:, t + 1, h, :] = norm
            den = jnp.sum(qf[sl] * norm, -1, keepdims=True)
            weight = jnp.ones((own, 1), F32)
            num = jnp.zeros((own, dim), F32)
            for s in range(t, -1, -1):
                ss = slice(s * own, (s + 1) * own)
                dots = jnp.sum(qf[sl] * kf[ss], -1, keepdims=True)
                num += (weight * admit[s][:, h : h + 1] * dots) * vf[ss]
                weight = weight * retain[s][:, h : h + 1]
            num += weight * base[sl]
            floor = jnp.exp(-stabs[t + 1][:, h : h + 1])
            rows.append(num / jnp.maximum(jnp.abs(den), floor))
        hidden = jnp.concatenate(rows, 0)
        outs.append(jax.nn.sigmoid(o.astype(F32)) * hidden)
    gated[...] = jnp.concatenate(outs, 1).astype(BF16)
    for t in range(props):
        coef[t] = jnp.concatenate([retain[t], admit[t]], 1)
    for t in range(props + 1):
        new_s[t] = stabs[t]


def memory_kernel(accepted, coef, m0, kv, out, *, heads):
    b = pl.program_id(0)
    _, steps, _, dim, _ = out.shape
    per = kv.shape[1]
    props = steps - 1
    own = per // props
    scale = dim ** (-0.5)
    for h in range(heads):
        key = kv[h].astype(F32) * scale
        value = kv[heads + h].astype(F32)
        memory = m0[0, 0, h]
        out[0, 0, h] = memory
        row = iota((per, dim), 0)
        keys = key.T
        for t in range(props):
            hit = row == t * own + b
            vrow = jnp.sum(jnp.where(hit, value, 0.0), 0, keepdims=True)
            lane = iota(keys.shape, 1)
            kcol = jnp.sum(jnp.where(lane == t * own + b, keys, 0.0), 1, keepdims=True)
            memory = coef[t, b, h] * memory + (coef[t, b, heads + h] * kcol) * vrow
            out[0, t + 1, h] = memory


def mix_kernel(gathered, w, out, *, owners, props):
    rows = gathered.shape[0]
    per = rows // owners
    own = per // props
    y = contract(w[...], gathered[...], 0, 1).astype(BF16)
    r, c = iota((rows, rows), 0), iota((rows, rows), 1)
    t, rest = c // (rows // props), c % (rows // props)
    source = (rest // own) * per + t * own + rest % own
    move = jnp.where(r == source, 1.0, 0.0).astype(BF16)
    y = contract(y, move, 1, 0).astype(BF16)
    out[...] = y.reshape(out.shape)


def finish_kernel(got, out):
    total = got[0].astype(F32)
    for k in range(1, got.shape[0]):
        total = total + got[k].astype(F32)
    props, _, seqs = out.shape
    for t in range(props):
        out[t] = total[:, t * seqs : (t + 1) * seqs].astype(BF16)


SMEM = pl.BlockSpec(memory_space=pltpu.SMEM)


def local(
    tokens,
    norm_gain,
    w_query,
    w_key,
    w_value,
    w_outgate,
    gate_weight,
    input_bias,
    forget_bias,
    w_out,
    saved_memory,
    saved_normalizer,
    saved_stabilizer,
    accepted,
):
    owners, peers = lax.axis_size("kv"), lax.axis_size("tp")
    seqs, props, width = tokens.shape
    heads = input_bias.shape[0]
    own, saved, _, dim, _ = saved_memory.shape
    columns = w_query.shape[1]
    per = own * props
    z = lax.axis_index("kv")
    place = jnp.stack([z, lax.axis_index("tp")]).astype(jnp.int32)
    blocks = 4 * columns // 128

    gates = gate_weight.transpose(0, 2, 1)
    all_heads = gates.shape[1]

    def whole(shape):
        return pl.BlockSpec(shape, lambda *_: (0,) * len(shape))

    send = pl.pallas_call(
        functools.partial(project_kernel, owners=owners),
        grid_spec=pltpu.PrefetchScalarGridSpec(
            num_scalar_prefetch=1,
            grid=(1,),
            in_specs=[
                whole(tokens.shape),
                whole((norm_gain.shape[0] // 128, 128)),
                pl.BlockSpec((2, all_heads, width), lambda i, p: (0, 0, p[0])),
            ]
            + [whole(w_query.shape)] * 4,
            out_specs=whole((owners, blocks * per + 8, 128)),
        ),
        out_shape=jax.ShapeDtypeStruct((owners, blocks * per + 8, 128), BF16),
        name="project",
    )(place, tokens, norm_gain.reshape(-1, 128), gates, w_query, w_key, w_value, w_outgate)

    got = lax.all_to_all(send, "kv", split_axis=0, concat_axis=0, tiled=True)

    rows_n = jnp.take_along_axis(saved_normalizer, accepted[:, None, None, None], 1)[:, 0]
    m0 = jnp.take_along_axis(saved_memory, accepted[:, None, None, None, None], 1)
    stab = saved_stabilizer.transpose(0, 2, 1)
    gated, kv, coef, new_n, new_s = pl.pallas_call(
        functools.partial(cell_kernel, features=float(owners * width)),
        in_specs=[SMEM] * 5 + [pl.BlockSpec(memory_space=pltpu.VMEM)] * 3,
        out_specs=[pl.BlockSpec(memory_space=pltpu.VMEM)] * 5,
        out_shape=[
            jax.ShapeDtypeStruct((per, columns), BF16),
            jax.ShapeDtypeStruct((2 * heads, per, dim), BF16),
            jax.ShapeDtypeStruct((props, own, 2 * heads), F32),
            jax.ShapeDtypeStruct((own, props + 1, heads, dim), F32),
            jax.ShapeDtypeStruct((props + 1, own, heads), F32),
        ],
        name="cell",
    )(place, accepted, stab, input_bias, forget_bias, got, m0, rows_n)

    gathered = lax.all_gather(gated, "kv", axis=0, tiled=True)

    terms = pl.pallas_call(
        functools.partial(mix_kernel, owners=owners, props=props),
        in_specs=[pl.BlockSpec(memory_space=pltpu.VMEM)] * 2,
        out_specs=pl.BlockSpec(memory_space=pltpu.VMEM),
        out_shape=jax.ShapeDtypeStruct((peers, w_out.shape[1] // peers, seqs * props), BF16),
        name="mix",
    )(gathered, w_out)
    arrived = lax.all_to_all(terms, "tp", split_axis=0, concat_axis=0, tiled=True)

    new_memory = pl.pallas_call(
        functools.partial(memory_kernel, heads=heads),
        grid_spec=pltpu.PrefetchScalarGridSpec(
            num_scalar_prefetch=1,
            grid=(own,),
            in_specs=[
                SMEM,
                pl.BlockSpec((1, 1, heads, dim, dim), lambda b, a: (b, a[b], 0, 0, 0)),
                whole((2 * heads, per, dim)),
            ],
            out_specs=pl.BlockSpec((1, props + 1, heads, dim, dim), lambda b, a: (b, 0, 0, 0, 0)),
        ),
        out_shape=jax.ShapeDtypeStruct((own, props + 1, heads, dim, dim), F32),
        cost_estimate=pl.CostEstimate(flops=10_000_000, bytes_accessed=3_200_000, transcendentals=0),
        name="memory",
    )(accepted, coef, saved_memory, kv)

    mixed = pl.pallas_call(
        finish_kernel,
        in_specs=[pl.BlockSpec(memory_space=pltpu.VMEM)],
        out_specs=pl.BlockSpec(memory_space=pltpu.VMEM),
        out_shape=jax.ShapeDtypeStruct((props, w_out.shape[1] // peers, seqs), BF16),
        name="finish",
    )(arrived)
    return mixed.transpose(2, 0, 1), new_memory, new_n, new_s.transpose(1, 0, 2)


def solution(mesh):
    return jax.shard_map(
        local,
        mesh=mesh,
        in_specs=(
            P("grp", None, "kv"),
            P(),
            P("kv", "tp"),
            P("kv", "tp"),
            P("kv", "tp"),
            P("kv", "tp"),
            P(),
            P("tp"),
            P("tp"),
            P("tp", "kv"),
            P(("grp", "kv"), None, "tp", None, None),
            P(("grp", "kv"), None, "tp", None),
            P(("grp", "kv"), None, "tp"),
            P(("grp", "kv")),
        ),
        out_specs=(
            P("grp", None, ("kv", "tp")),
            P(("grp", "kv"), None, "tp", None, None),
            P(("grp", "kv"), None, "tp", None),
            P(("grp", "kv"), None, "tp"),
        ),
        check_vma=False,
    )
```

time: 149 us -> 113 us (0.76)
  waiting for transfers between devices: 58.8 us -> 18.7 us
  blocking collectives: 0 us -> 28.5 us
  local copies, waits for them, and re-layouts: 20.5 us -> 5.76 us
  Pallas kernels: 0 us -> 14.6 us
  matrix products: 10.4 us -> 0 us
  other arithmetic: 11.7 us -> 2.88 us
  starting transfers between devices: 45.7 us -> 41.6 us
    all_to_all x3 -> x2, waiting for transfers between devices: 58.8 us -> 18.7 us  [the longest x1 18.7 us: local(): got = lax.all_to_all(send, 'kv', split_axis=0, concat_axis=0, tiled=True)]
    all_gather x0 -> x1, blocking collectives: none -> 28.5 us  [local(): gathered = lax.all_gather(gated, 'kv', axis=0, tiled=True)]
    pallas_call x0 -> x5, Pallas kernels: none -> 14.6 us  [the longest x1 4.85 us: local(): pl.pallas_call(functools.partial(memory_kernel, heads=heads), grid_spec=p...]
    concatenate x10 -> x0, local copies, waits for them, and re-layouts: 12.5 us -> none  [sent_together(): jnp.concatenate([a.reshape(*a.shape[:along], w) for a, w in zip(arrays, w...]
    dot_general x11 -> x0, matrix products: 10.4 us -> none  [the longest x6 7.78 us: local_term(): jnp.dot(scaled, weight, preferred_element_type=jnp.float32)]
    unnamed x8 -> x0, other arithmetic: 4.82 us -> none
    all_to_all x3 -> x2, starting transfers between devices: 45.7 us -> 41.6 us  [the longest x1 24.5 us: local(): got = lax.all_to_all(send, 'kv', split_axis=0, concat_axis=0, tiled=True)]
    reduce_sum x4 -> x0, other arithmetic: 3.38 us -> none  [the longest x1 1.46 us: summed_on_arrival(): return arrived.sum(axis=0)]
  transfers between devices with their start and end apart: 3 -> 2, of which waited for: 3 -> 1; matrix products, arithmetic and copies ran while one was open for 6% -> 6% of each run, Pallas kernels for 0% -> 4%
where the time goes in v1:
time: 113 us
  starting transfers between devices  41.6 us (37%)
  blocking collectives  28.5 us (25%)
  waiting for transfers between devices  18.7 us (17%)
  Pallas kernels  14.6 us (13%)
  local copies, waits for them, and re-layouts  5.76 us (5%)
  other arithmetic  2.88 us (3%)
    all_gather x1, blocking collectives, local(): gathered = lax.all_gather(gated, 'kv', axis=0, tiled=True)  28.5 us
    all_to_all x1, starting transfers between devices, local(): got = lax.all_to_all(send, 'kv', split_axis=0, concat_axis=0, tiled=True)  24.5 us
    all_to_all x1, waiting for transfers between devices, local(): got = lax.all_to_all(send, 'kv', split_axis=0, concat_axis=0, tiled=True)  18.7 us
    all_to_all x1, starting transfers between devices, local(): lax.all_to_all(terms, 'tp', split_axis=0, concat_axis=0, tiled=True)  17.1 us
    pallas_call x1, Pallas kernels, local(): pl.pallas_call(functools.partial(memory_kernel, heads=heads), grid_spec=p...  4.85 us
    pallas_call x1, Pallas kernels, local(): pl.pallas_call(functools.partial(project_kernel, owners=owners), grid_spe...  3.6 us
    unnamed x10, local copies, waits for them, and re-layouts  2.86 us
    pallas_call x1, Pallas kernels, local(): pl.pallas_call(functools.partial(cell_kernel, features=float(owners * wid...  2.6 us
  transfers between devices with their start and end apart: 2, of which 1 were waited for; matrix products, arithmetic and copies ran while one was open for 6% of the time, Pallas kernels for 4%

profile of v1, /device:TPU:33, one launch (start us, length us, event | category | flops | bytes accessed | tf_op | source)
XLA Modules:
  0.0 112.7 jit_solution(8731031690390282665)
XLA Ops:
  0.6 0.0 copy-start
  0.6 0.0 copy-start.3
  0.7 0.6 pad_add_fusion.place
  1.3 3.6 %project.1 = bf16[16,136,128]{2,1,0:T(8,128)(2,1)} custom-call(s32[2]{0:T(128)} %pad_add_fusion.place, bf16[64,4,256]{2,1,0:T(4,128)(2,1)} %tokens.1, bf16[32,128]{1,0:T(8,128)(2,1)} %bitcast.18, bf16[2,16,4096]{2,1,0:T(8,128)(2,1)} %bitcast.15, bf16[256,256]{1,0:T(8,128)(2,1)} %wq.1, bf16[256,256]{1,0:T(8,128)(2,1)} %wk.1, bf16[256,256]{1,0:T(8,128)(2,1)} %wv.1, ...), custom_call_target="tpu_custom_call" | custom-call | tf_op jit(solution)/shard_map/project/pallas_call | solution.py:241
  4.9 24.5 %all-to-all-start = ((bf16[16,136,128]{2,1,0:T(8,128)(2,1)}), bf16[16,136,128]{2,1,0:T(8,128)(2,1)S(1)}, u32[]{:S(2)}, u32[]{:S(2)}) async-start(bf16[16,136,128]{2,1,0:T(8,128)(2,1)} %project.1), calls=%async_computation | async-start | bytes 1114112 | tf_op jit(solution)/shard_map/all_to_all | solution.py:258
  29.4 0.7 fusion
  30.1 0.0 copy-done
  30.1 0.6 gather_fusion.1
  30.7 2.3 %gather_fusion = f32[4,2,128,128]{3,2,1,0:T(8,128)S(1)} fusion(f32[4,5,2,128,128]{4,3,2,1,0:T(8,128)} %m0.1, s32[4]{0:T(128)S(1)} %or_bitcast_fusion), kind=kCustom, calls=%fused_computation | custom fusion | bytes 1048608 | tf_op jit(solution)/shard_map/jit(take_along_axis)/gather | solution.py:261
  33.0 0.0 copy-done.3
  33.0 0.7 broadcast_select_fusion.n0
  33.7 0.9 bitcast_select_fusion.m0
  34.6 18.7 %all-to-all-done.got = bf16[16,136,128]{2,1,0:T(8,128)(2,1)S(1)} async-done(((bf16[16,136,128]{2,1,0:T(8,128)(2,1)}), bf16[16,136,128]{2,1,0:T(8,128)(2,1)S(1)}, u32[]{:S(2)}, u32[]{:S(2)}) %all-to-all-start) | async-done | bytes 557088 | tf_op jit(solution)/shard_map/all_to_all | solution.py:258
  53.3 0.0 copy-start.1
  53.3 0.8 copy-done.1
  54.1 2.6 %cell.1 = (bf16[16,256]{1,0:T(8,128)(2,1)}, bf16[4,16,128]{2,1,0:T(8,128)(2,1)}, f32[4,4,4]{2,1,0:T(4,128)}, f32[4,5,2,128]{3,2,1,0:T(2,128)}, f32[5,4,2]{2,1,0:T(4,128)}) custom-call(s32[2]{0:T(128)} %pad_add_fusion.place, s32[4]{0:T(128)} %accepted.3, f32[4,2,5]{2,1,0:T(2,128)} %bitcast.19, f32[2]{0:T(128)} %ib.1, f32[2]{0:T(128)} %fb.1, ...), custom_call_target="tpu_custom_call" | custom-call | tf_op jit(solution)/shard_map/cell/pallas_call | solution.py:263
  56.7 28.5 %all_gather.3.gathered = bf16[256,256]{1,0:T(8,128)(2,1)} all-gather(bf16[16,256]{1,0:T(8,128)(2,1)} %get-tuple-element.9), channel_id=1, replica_groups=mesh['grp'=2,'kv'=16,'tp'=8] {'kv'}, dimensions={0}, use_global_device_ids=true | all-gather | bytes 139264 | tf_op jit(solution)/shard_map/all_gather | solution.py:277
  85.2 2.0 %mix.1 = bf16[8,32,256]{2,1,0:T(8,128)(2,1)} custom-call(bf16[256,256]{1,0:T(8,128)(2,1)} %all_gather.3.gathered, bf16[256,256]{1,0:T(8,128)(2,1)} %w.1), custom_call_target="tpu_custom_call" | custom-call | tf_op jit(solution)/shard_map/mix/pallas_call | solution.py:279
  87.2 17.1 %all-to-all-start.1 = ((bf16[8,32,256]{2,1,0:T(8,128)(2,1)}), bf16[8,32,256]{2,1,0:T(8,128)(2,1)S(1)}, u32[]{:S(2)}, u32[]{:S(2)}) async-start(bf16[8,32,256]{2,1,0:T(8,128)(2,1)} %mix.1), calls=%async_computation.1 | async-start | bytes 262144 | tf_op jit(solution)/shard_map/all_to_all | solution.py:286
  104.2 1.4 %copy.18 = f32[4,5,2]{1,2,0:T(2,128)} copy(f32[4,5,2]{2,0,1:T(4,128)} %bitcast.17) | data formatting | bytes 320
  105.6 4.8 %memory.1 = f32[4,5,2,128,128]{4,3,2,1,0:T(8,128)} custom-call(s32[4]{0:T(128)} %accepted.3, f32[4,4,4]{2,1,0:T(4,128)} %get-tuple-element.10.coef, f32[4,5,2,128,128]{4,3,2,1,0:T(8,128)} %m0.1, bf16[4,16,128]{2,1,0:T(8,128)(2,1)} %get-tuple-element.11.kv), custom_call_target="tpu_custom_call" | custom-call | flops 10000000 | bytes 3200000 | tf_op jit(solution)/shard_map/memory/pallas_call | solution.py:288
  110.5 0.0 all-to-all-done.1.got
  110.5 0.0 copy-start.2
  110.5 0.6 copy-done.2
  111.1 1.6 %finish.1 = bf16[4,32,64]{2,1,0:T(8,128)(2,1)} custom-call(bf16[8,32,256]{2,1,0:T(8,128)(2,1)} %copy-done.2), custom_call_target="tpu_custom_call" | custom-call | tf_op jit(solution)/shard_map/finish/pallas_call | solution.py:305
  (4 shorter events, 0.0 us)
Async XLA Ops:
  0.6 29.5 %copy-start = (f32[4,5,2,128]{3,2,1,0:T(2,128)S(1)}, f32[4,5,2,128]{3,2,1,0:T(2,128)}, u32[]{:S(2)}) copy-start(f32[4,5,2,128]{3,2,1,0:T(2,128)} %param.25) | copy-start | bytes 61444
  0.6 32.4 %copy-start.3 = (s32[4]{0:T(128)S(1)}, s32[4]{0:T(128)}, u32[]{:S(2)}) copy-start(s32[4]{0:T(128)} %accepted.3) | copy-start | bytes 52
  4.9 48.4 %all-to-all-start = ((bf16[16,136,128]{2,1,0:T(8,128)(2,1)}), bf16[16,136,128]{2,1,0:T(8,128)(2,1)S(1)}, u32[]{:S(2)}, u32[]{:S(2)}) async-start(bf16[16,136,128]{2,1,0:T(8,128)(2,1)} %project.1), calls=%async_computation | async-start | bytes 1114112 | tf_op jit(solution)/shard_map/all_to_all | solution.py:258
  53.3 0.8 copy-start.1
  87.2 23.3 %all-to-all-start.1 = ((bf16[8,32,256]{2,1,0:T(8,128)(2,1)}), bf16[8,32,256]{2,1,0:T(8,128)(2,1)S(1)}, u32[]{:S(2)}, u32[]{:S(2)}) async-start(bf16[8,32,256]{2,1,0:T(8,128)(2,1)} %mix.1), calls=%async_computation.1 | async-start | bytes 262144 | tf_op jit(solution)/shard_map/all_to_all | solution.py:286
  110.5 0.7 copy-start.2

commit v2 on v1

v2 whole, which is shorter than its diff:
```python
import functools

import jax
import jax.numpy as jnp
from jax import lax
from jax.experimental import pallas as pl
from jax.experimental.pallas import tpu as pltpu
from jax.sharding import PartitionSpec as P

EPSILON = 1e-06
F32 = jnp.float32
BF16 = jnp.bfloat16
SHIFT = 2.0**20


def iota(shape, dim):
    return lax.broadcasted_iota(jnp.int32, shape, dim)


def contract(a, b, da, db):
    return lax.dot_general(a, b, (((da,), (db,)), ((), ())), preferred_element_type=F32)


def coded(x):
    y = x * SHIFT
    return ((y * jnp.abs(y)) * (y * y)).astype(BF16)


def decoded(y):
    y = y.astype(F32)
    root = lax.rsqrt(lax.rsqrt(jnp.maximum(jnp.abs(y), 1e-37)))
    return jnp.where(y < 0.0, -root, root)


def project_kernel(tokens, gain, wq, wk, wv, wo, gates_hbm, out, gates, sem, *, owners):
    z, tp = lax.axis_index("kv"), lax.axis_index("tp")
    seqs, props, width = tokens.shape
    fetch = pltpu.make_async_copy(gates_hbm.at[:, :, pl.ds(pl.multiple_of(z * width, width), width)], gates, sem)
    fetch.start()
    rows = seqs * props
    per = rows // owners
    own = per // props
    x = tokens[...].astype(F32).reshape(rows, width)
    gain_rows = gain[...].astype(F32)
    pieces = []
    for j in range(width // 128):
        hit = iota(gain_rows.shape, 0) == z * (width // 128) + j
        pieces.append(jnp.sum(jnp.where(hit, gain_rows, 0.0), 0, keepdims=True))
    scaled = (x * jnp.concatenate(pieces, 1)).astype(BF16)
    r, c = iota((rows, rows), 0), iota((rows, rows), 1)
    source = (r & -per) + (r & (own - 1)) * props + ((r & (per - 1)) >> log2(own))
    move = jnp.where(c == source, 1.0, 0.0).astype(BF16)
    scaled = contract(move, scaled, 1, 0).astype(BF16)
    block = 0
    for w in (wq, wk, wv, wo):
        y = coded(contract(scaled, w[...], 1, 0))
        for h in range(y.shape[1] // 128):
            out[:, block * per : (block + 1) * per, :] = y[:, h * 128 : (h + 1) * 128].reshape(owners, per, 128)
            block += 1
    square = x * x
    s_hi = square.astype(BF16)
    s_lo = (square - s_hi.astype(F32)).astype(BF16)
    ones = jnp.ones((8, width), BF16)
    s = contract(ones, contract(move, s_hi, 1, 0).astype(BF16), 1, 1)
    s += contract(ones, contract(move, s_lo, 1, 0).astype(BF16), 1, 1)
    fetch.wait()
    heads = gates.shape[1]
    local = heads // lax.axis_size("tp")
    pick_r, pick_c = iota((8, 2 * heads), 0), iota((8, 2 * heads), 1)
    want = ((pick_r & 3) // local) * heads + tp * local + (pick_r & (local - 1))
    pick = jnp.where(pick_c == want, 1.0, 0.0).astype(BF16)
    own_gates = contract(pick, gates[...].reshape(2 * heads, width), 1, 0).astype(BF16)
    g = contract(own_gates, scaled, 1, 1)

    def words(value, split):
        hi = value.astype(BF16).astype(F32)
        return jnp.where(iota(value.shape, 0) < split, hi, value - hi)

    g, s = words(g, 4), words(s, 1)
    lanes = iota((8, 128), 1)
    span = 128 // per
    for half in range(rows // 128):
        gh = g[:, half * 128 : (half + 1) * 128]
        sh = pltpu.roll(s[:, half * 128 : (half + 1) * 128], 64, 1)
        low = jnp.where(lanes < 64, gh, sh).astype(BF16)
        high = jnp.where(lanes < 64, sh, gh).astype(BF16)
        for k in range(span):
            out[half * span + k, block * per :, :] = low if k < span // 2 else high


def cell_kernel(accepted, stab, ib, fb, got, m0, n0, gated, kv_out, coef, *, features):
    z = lax.axis_index("kv")
    owners = got.shape[0]
    own, _, heads, dim, _ = m0.shape
    main = got.shape[1] - 8
    per = main // (4 * heads)
    props = per // own
    small = got[0, main:].astype(F32)
    for k in range(1, owners):
        small = small + got[k, main:].astype(F32)
    shift = (z & (128 // per - 1)) * per
    small = pltpu.roll(small, (128 - shift) & 127, 1)
    g = small + pltpu.roll(small, 4, 0)
    sq = pltpu.roll(small + pltpu.roll(small, 7, 0), 64, 1)
    packed = jnp.where(iota(g.shape, 0) < 4, g, pltpu.roll(sq, 4, 0))
    cols = packed.T[:per]
    inverse = lax.rsqrt(cols[:, 4:5] / features + EPSILON)
    col = iota((per, heads), 1)
    ibv, fbv = jnp.zeros((per, heads), F32), jnp.zeros((per, heads), F32)
    for h in range(heads):
        ibv, fbv = jnp.where(col == h, ib[h], ibv), jnp.where(col == h, fb[h], fbv)
    in_gate = cols[:, 0:2] * inverse + ibv
    f = cols[:, 2:4] * inverse + fbv
    log_forget = jnp.minimum(f, 0.0) - jnp.log1p(jnp.exp(-jnp.abs(f)))
    srow, scol = iota((own, heads), 0), iota((own, heads), 1)
    m = jnp.zeros((own, heads), F32)
    for b in range(own):
        for h in range(heads):
            m = jnp.where((srow == b) & (scol == h), stab[b, h, accepted[b]], m)
    stabs, retain, admit = [m], [], []
    for t in range(props):
        carried = log_forget[t * own : (t + 1) * own] + m
        incoming = in_gate[t * own : (t + 1) * own]
        top = jnp.maximum(carried, incoming)
        retain.append(jnp.exp(carried - top))
        admit.append(jnp.exp(incoming - top))
        m = top
        stabs.append(m)
    scale = dim ** (-0.5)
    factor = inverse * (1.0 / SHIFT)
    rr = iota((per, dim), 0) & (own - 1)

    def part(kind, h):
        rows = slice((kind * heads + h) * per, (kind * heads + h + 1) * per)
        total = decoded(got[0, rows])
        for k in range(1, owners):
            total = total + decoded(got[k, rows])
        return (total * factor).astype(BF16)

    outs = []
    for h in range(heads):
        q, k, v, o = part(0, h), part(1, h), part(2, h), part(3, h)
        kv_out[h] = k
        kv_out[heads + h] = v
        qf, kf, vf = q.astype(F32), k.astype(F32) * scale, v.astype(F32)
        base = jnp.zeros((per, dim), F32)
        for b in range(own):
            mine = jnp.where(rr == b, qf, 0.0).astype(BF16)
            mem = m0[b, 0, h]
            hi = mem.astype(BF16)
            lo = (mem - hi.astype(F32)).astype(BF16)
            base += contract(mine, hi, 1, 0) + contract(mine, lo, 1, 0)
        norm = n0[:, h, :]
        rows = []
        for t in range(props):
            sl = slice(t * own, (t + 1) * own)
            norm = retain[t][:, h : h + 1] * norm + admit[t][:, h : h + 1] * kf[sl]
            den = jnp.sum(qf[sl] * norm, -1, keepdims=True)
            weight = jnp.ones((own, 1), F32)
            num = jnp.zeros((own, dim), F32)
            for s in range(t, -1, -1):
                ss = slice(s * own, (s + 1) * own)
                dots = jnp.sum(qf[sl] * kf[ss], -1, keepdims=True)
                num += (weight * admit[s][:, h : h + 1] * dots) * vf[ss]
                weight = weight * retain[s][:, h : h + 1]
            num += weight * base[sl]
            floor = jnp.exp(-stabs[t + 1][:, h : h + 1])
            rows.append(num / jnp.maximum(jnp.abs(den), floor))
        hidden = jnp.concatenate(rows, 0)
        outs.append(jax.nn.sigmoid(o.astype(F32)) * hidden)
    both = jnp.concatenate(outs, 1).astype(BF16)
    for k in range(gated.shape[0]):
        gated[k] = both
    for t in range(props + 1):
        last = t - 1 if t else 0
        coef[t] = jnp.concatenate([stabs[t], retain[last], admit[last]], 1)


def memory_kernel(accepted, coef, m0, n0, kv, new_m, new_n, new_s, *, heads):
    b = pl.program_id(0)
    _, steps, _, dim, _ = new_m.shape
    per = kv.shape[1]
    props = steps - 1
    own = per // props
    scale = dim ** (-0.5)
    row, col = iota((heads, steps), 0), iota((heads, steps), 1)
    stabs = jnp.zeros((heads, steps), F32)
    for h in range(heads):
        for t in range(steps):
            stabs = jnp.where((row == h) & (col == t), coef[t, b, h], stabs)
        key = kv[h].astype(F32) * scale
        value = kv[heads + h].astype(F32)
        memory, norm = m0[0, 0, h], n0[0, 0, h : h + 1]
        new_m[0, 0, h] = memory
        new_n[0, 0, h : h + 1] = norm
        row_at = iota((per, dim), 0)
        keys = key.T
        lane = iota(keys.shape, 1)
        for t in range(props):
            keep, add = coef[t + 1, b, heads + h], coef[t + 1, b, 2 * heads + h]
            at = t * own + b
            vrow = jnp.sum(jnp.where(row_at == at, value, 0.0), 0, keepdims=True)
            krow = jnp.sum(jnp.where(row_at == at, key, 0.0), 0, keepdims=True)
            kcol = jnp.sum(jnp.where(lane == at, keys, 0.0), 1, keepdims=True)
            memory = keep * memory + (add * kcol) * vrow
            norm = keep * norm + add * krow
            new_m[0, t + 1, h] = memory
            new_n[0, t + 1, h : h + 1] = norm
    new_s[0] = stabs


def mix_kernel(gathered, w, after, out):
    owners, per, _ = gathered.shape
    rows = owners * per
    y = contract(w[...], gathered[...].reshape(rows, gathered.shape[2]), 0, 1).astype(BF16)
    out[...] = y.reshape(out.shape)


def finish_kernel(got, out, *, owners):
    total = got[0].astype(F32)
    for k in range(1, got.shape[0]):
        total = total + got[k].astype(F32)
    props, _, seqs = out.shape
    rows = props * seqs
    per = rows // owners
    own = per // props
    r, c = iota((rows, rows), 0), iota((rows, rows), 1)
    t, rest = c >> log2(seqs), c & (seqs - 1)
    source = (rest >> log2(own)) * per + t * own + (rest & (own - 1))
    move = jnp.where(r == source, 1.0, 0.0).astype(BF16)
    y = contract(total.astype(BF16), move, 1, 0).astype(BF16)
    for t in range(props):
        out[t] = y[:, t * seqs : (t + 1) * seqs]


def log2(n):
    assert n & (n - 1) == 0
    return n.bit_length() - 1


SMEM = pl.BlockSpec(memory_space=pltpu.SMEM)
VMEM = pl.BlockSpec(memory_space=pltpu.VMEM)


def held(shape, dtype):
    return pltpu.VMEM(shape, dtype)


def near(x):
    return pltpu.with_memory_space_constraint(x, pltpu.VMEM)


def local(
    tokens,
    norm_gain,
    w_query,
    w_key,
    w_value,
    w_outgate,
    gate_weight,
    input_bias,
    forget_bias,
    w_out,
    saved_memory,
    saved_normalizer,
    saved_stabilizer,
    accepted,
):
    owners, peers = lax.axis_size("kv"), lax.axis_size("tp")
    seqs, props, width = tokens.shape
    heads = input_bias.shape[0]
    own, saved, _, dim, _ = saved_memory.shape
    columns = w_query.shape[1]
    per = own * props
    blocks = 4 * columns // 128
    gates = gate_weight.transpose(0, 2, 1)
    all_heads = gates.shape[1]

    def whole(shape):
        return pl.BlockSpec(shape, lambda *_: (0,) * len(shape))

    send = pl.pallas_call(
        functools.partial(project_kernel, owners=owners),
        in_specs=[VMEM] * 6 + [pl.BlockSpec(memory_space=pl.ANY)],
        out_specs=[VMEM],
        out_shape=[held((owners, blocks * per + 8, 128), BF16)],
        scratch_shapes=[pltpu.VMEM((2, all_heads, width), BF16), pltpu.SemaphoreType.DMA],
        name="project",
    )(tokens, norm_gain.reshape(-1, 128), w_query, w_key, w_value, w_outgate, gates)[0]

    got = lax.all_to_all(send, "kv", split_axis=0, concat_axis=0, tiled=True)

    n0 = jnp.take_along_axis(saved_normalizer, accepted[:, None, None, None], 1)[:, 0]
    m0 = jnp.take_along_axis(saved_memory, accepted[:, None, None, None, None], 1)
    stab = saved_stabilizer.transpose(0, 2, 1)
    steps = props + 1
    gated, kv, coef = pl.pallas_call(
        functools.partial(cell_kernel, features=float(owners * width)),
        in_specs=[SMEM] * 4 + [VMEM] * 3,
        out_specs=[VMEM] * 3,
        out_shape=[
            held((owners, per, columns), BF16),
            held((2 * heads, per, dim), BF16),
            jax.ShapeDtypeStruct((steps, own, 3 * heads), F32),
        ],
        name="cell",
    )(accepted, stab, input_bias, forget_bias, near(got), near(m0), near(n0))

    gathered = lax.all_to_all(gated, "kv", split_axis=0, concat_axis=0, tiled=True)

    new_memory, new_n, new_s = pl.pallas_call(
        functools.partial(memory_kernel, heads=heads),
        grid_spec=pltpu.PrefetchScalarGridSpec(
            num_scalar_prefetch=1,
            grid=(own,),
            in_specs=[
                SMEM,
                pl.BlockSpec((1, 1, heads, dim, dim), lambda b, a: (b, a[b], 0, 0, 0)),
                pl.BlockSpec((1, 1, heads, dim), lambda b, a: (b, a[b], 0, 0)),
                whole((2 * heads, per, dim)),
            ],
            out_specs=[
                pl.BlockSpec((1, steps, heads, dim, dim), lambda b, a: (b, 0, 0, 0, 0)),
                pl.BlockSpec((1, steps, heads, dim), lambda b, a: (b, 0, 0, 0)),
                pl.BlockSpec((1, heads, steps), lambda b, a: (b, 0, 0)),
            ],
        ),
        out_shape=[
            jax.ShapeDtypeStruct((own, steps, heads, dim, dim), F32),
            jax.ShapeDtypeStruct((own, steps, heads, dim), F32),
            jax.ShapeDtypeStruct((own, heads, steps), F32),
        ],
        cost_estimate=pl.CostEstimate(flops=20_000_000, bytes_accessed=3_200_000, transcendentals=0),
        name="memory",
    )(accepted, coef, saved_memory, saved_normalizer, near(kv))

    terms = pl.pallas_call(
        mix_kernel,
        in_specs=[VMEM] * 2 + [pl.BlockSpec(memory_space=pl.ANY)],
        out_specs=[VMEM],
        out_shape=[held((peers, w_out.shape[1] // peers, seqs * props), BF16)],
        name="mix",
    )(near(gathered), near(w_out), new_s)[0]
    arrived = lax.all_to_all(terms, "tp", split_axis=0, concat_axis=0, tiled=True)

    mixed = pl.pallas_call(
        functools.partial(finish_kernel, owners=owners),
        in_specs=[VMEM],
        out_specs=VMEM,
        out_shape=jax.ShapeDtypeStruct((props, w_out.shape[1] // peers, seqs), BF16),
        name="finish",
    )(near(arrived))
    return mixed.transpose(2, 0, 1), new_memory, new_n, new_s.transpose(0, 2, 1)


def solution(mesh):
    return jax.shard_map(
        local,
        mesh=mesh,
        in_specs=(
            P("grp", None, "kv"),
            P(),
            P("kv", "tp"),
            P("kv", "tp"),
            P("kv", "tp"),
            P("kv", "tp"),
            P(),
            P("tp"),
            P("tp"),
            P("tp", "kv"),
            P(("grp", "kv"), None, "tp", None, None),
            P(("grp", "kv"), None, "tp", None),
            P(("grp", "kv"), None, "tp"),
            P(("grp", "kv")),
        ),
        out_specs=(
            P("grp", None, ("kv", "tp")),
            P(("grp", "kv"), None, "tp", None, None),
            P(("grp", "kv"), None, "tp", None),
            P(("grp", "kv"), None, "tp"),
        ),
        check_vma=False,
    )
```

time: 113 us -> 94 us (0.83)
  blocking collectives: 28.5 us -> 13.1 us
  waiting for transfers between devices: 18.7 us -> 26.2 us
  starting transfers between devices: 41.6 us -> 37.6 us
  Pallas kernels: 14.6 us -> 11.3 us
  local copies, waits for them, and re-layouts: 5.76 us -> 3.64 us
  other arithmetic: 2.88 us -> 0.87 us
    all_gather x1 -> x0, blocking collectives: 28.5 us -> none  [local(): gathered = lax.all_gather(gated, 'kv', axis=0, tiled=True)]
    all_to_all x0 -> x1, blocking collectives: none -> 13.1 us  [local(): lax.all_to_all(terms, 'tp', split_axis=0, concat_axis=0, tiled=True)]
    all_to_all x1, waiting for transfers between devices: 0.01 us -> 6.88 us  [local(): lax.all_to_all(gated, 'kv', split_axis=0, concat_axis=0, tiled=True)]
    all_to_all x1, starting transfers between devices: 17.1 us -> 13 us  [local(): lax.all_to_all(gated, 'kv', split_axis=0, concat_axis=0, tiled=True)]
    pallas_call x3, Pallas kernels: 7.2 us -> 4.08 us  [the longest x1 3.01 us: local(): pl.pallas_call(functools.partial(project_kernel, owners=owners), in_specs...]
    unnamed x10 -> x5, local copies, waits for them, and re-layouts: 2.86 us -> 0.02 us
  transfers between devices with their start and end apart: 2 -> 2, of which waited for: 1 -> 2; matrix products, arithmetic and copies ran while one was open for 6% -> 5% of each run, Pallas kernels for 4% -> 5%
where the time goes in v2:
time: 94 us; the launch traced here: 93.4 us
  starting transfers between devices  37.6 us (40%)
  waiting for transfers between devices  26.2 us (28%)
  blocking collectives  13.1 us (14%)
  Pallas kernels  11.3 us (12%)
  local copies, waits for them, and re-layouts  3.64 us (4%)
    all_to_all x1, starting transfers between devices, local(): got = lax.all_to_all(send, 'kv', split_axis=0, concat_axis=0, tiled=True)  24.5 us
    all_to_all x1, waiting for transfers between devices, local(): got = lax.all_to_all(send, 'kv', split_axis=0, concat_axis=0, tiled=True)  19.3 us
    all_to_all x1, blocking collectives, local(): lax.all_to_all(terms, 'tp', split_axis=0, concat_axis=0, tiled=True)  13.1 us
    all_to_all x1, starting transfers between devices, local(): lax.all_to_all(gated, 'kv', split_axis=0, concat_axis=0, tiled=True)  13 us
    all_to_all x1, waiting for transfers between devices, local(): lax.all_to_all(gated, 'kv', split_axis=0, concat_axis=0, tiled=True)  6.88 us
    pallas_call x1, Pallas kernels, local(): pl.pallas_call(functools.partial(memory_kernel, heads=heads), grid_spec=p...  4.9 us
    pallas_call x1, Pallas kernels, local(): pl.pallas_call(functools.partial(project_kernel, owners=owners), in_specs...  3.01 us
    gather x1, local copies, waits for them, and re-layouts, local(): jnp.take_along_axis(saved_memory, accepted[:, None, None, None, None], 1)  2.32 us
  transfers between devices with their start and end apart: 2, of which 2 were waited for; matrix products, arithmetic and copies ran while one was open for 5% of the time, Pallas kernels for 5%

profile of v2, /device:TPU:33, one launch (start us, length us, event | category | flops | bytes accessed | tf_op | source)
XLA Modules:
  0.0 93.4 jit_solution(8338399748168066802)
XLA Ops:
  0.6 0.0 copy-start.1
  0.6 3.0 %project.1 = bf16[16,136,128]{2,1,0:T(8,128)(2,1)} custom-call(bf16[64,4,256]{2,1,0:T(4,128)(2,1)} %tokens.1, bf16[32,128]{1,0:T(8,128)(2,1)} %bitcast.15, bf16[256,256]{1,0:T(8,128)(2,1)} %wq.1, bf16[256,256]{1,0:T(8,128)(2,1)} %wk.1, bf16[256,256]{1,0:T(8,128)(2,1)} %wv.1, bf16[256,256]{1,0:T(8,128)(2,1)} %wo.1, bf16[2,16,4096]{2,1,0:T(8,128)(2,1)} %bitcast.13), custom_call_target="tpu_custom_call" | custom-call | tf_op jit(solution)/shard_map/project/pallas_call | solution.py:282
  3.7 24.5 %all-to-all-start = ((bf16[16,136,128]{2,1,0:T(8,128)(2,1)}), bf16[16,136,128]{2,1,0:T(8,128)(2,1)S(1)}, u32[]{:S(2)}, u32[]{:S(2)}) async-start(bf16[16,136,128]{2,1,0:T(8,128)(2,1)} %project.1), calls=%async_computation | async-start | bytes 1114112 | tf_op jit(solution)/shard_map/all_to_all | solution.py:291
  28.2 0.7 fusion
  28.9 1.3 %gather_fusion.1 = f32[4,2,128]{2,1,0:T(2,128)S(1)} fusion(f32[4,5,2,128]{3,2,1,0:T(2,128)} %n0.1, s32[4]{0:T(128)S(1)} %or_bitcast_fusion), kind=kCustom, calls=%fused_computation.1 | custom fusion | bytes 8224 | tf_op jit(solution)/shard_map/jit(take_along_axis)/gather | solution.py:293
  30.2 2.3 %gather_fusion = f32[4,2,128,128]{3,2,1,0:T(8,128)S(1)} fusion(f32[4,5,2,128,128]{4,3,2,1,0:T(8,128)} %m0.1, s32[4]{0:T(128)S(1)} %or_bitcast_fusion), kind=kCustom, calls=%fused_computation | custom fusion | bytes 1048608 | tf_op jit(solution)/shard_map/jit(take_along_axis)/gather | solution.py:294
  32.5 0.0 copy-done.1
  32.5 0.0 copy-start
  32.6 0.1 broadcast_select_fusion.n0
  32.6 0.1 bitcast_select_fusion.m0
  32.7 19.3 %all-to-all-done.got = bf16[16,136,128]{2,1,0:T(8,128)(2,1)S(1)} async-done(((bf16[16,136,128]{2,1,0:T(8,128)(2,1)}), bf16[16,136,128]{2,1,0:T(8,128)(2,1)S(1)}, u32[]{:S(2)}, u32[]{:S(2)}) %all-to-all-start) | async-done | bytes 557088 | tf_op jit(solution)/shard_map/all_to_all | solution.py:291
  52.1 2.3 %cell.1 = (bf16[16,16,256]{2,1,0:T(8,128)(2,1)}, bf16[4,16,128]{2,1,0:T(8,128)(2,1)S(1)}, f32[5,4,6]{2,1,0:T(4,128)}) custom-call(s32[4]{0:T(128)} %accepted.3, f32[4,2,5]{2,1,0:T(2,128)} %bitcast.16, f32[2]{0:T(128)} %ib.1, f32[2]{0:T(128)} %fb.1, bf16[16,136,128]{2,1,0:T(8,128)(2,1)S(1)} %all-to-all-done.got, ...), custom_call_target="tpu_custom_call" | custom-call | tf_op jit(solution)/shard_map/cell/pallas_call | solution.py:297
  54.4 13.0 %all-to-all-start.1 = ((bf16[16,16,256]{2,1,0:T(8,128)(2,1)}), bf16[16,16,256]{2,1,0:T(8,128)(2,1)S(1)}, u32[]{:S(2)}, u32[]{:S(2)}) async-start(bf16[16,16,256]{2,1,0:T(8,128)(2,1)} %get-tuple-element.10), calls=%async_computation.1 | async-start | bytes 262144 | tf_op jit(solution)/shard_map/all_to_all | solution.py:309
  67.4 4.9 %memory.1 = (f32[4,5,2,128,128]{4,3,2,1,0:T(8,128)}, f32[4,5,2,128]{3,2,1,0:T(2,128)}, f32[4,2,5]{2,1,0:T(2,128)}) custom-call(s32[4]{0:T(128)} %accepted.3, f32[5,4,6]{2,1,0:T(4,128)} %get-tuple-element.11.coef, f32[4,5,2,128,128]{4,3,2,1,0:T(8,128)} %m0.1, f32[4,5,2,128]{3,2,1,0:T(2,128)} %n0.1, bf16[4,16,128]{2,1,0:T(8,128)(2,1)S(1)} %get-tuple-element.12.kv), custom_call_target="tpu_custom_call" | custom-call | flops 20000000 | bytes 3200000 | tf_op jit(solution)/shard_map/memory/pallas_call | solution.py:311
  72.3 6.9 %all-to-all-done.1.gathered = bf16[16,16,256]{2,1,0:T(8,128)(2,1)S(1)} async-done(((bf16[16,16,256]{2,1,0:T(8,128)(2,1)}), bf16[16,16,256]{2,1,0:T(8,128)(2,1)S(1)}, u32[]{:S(2)}, u32[]{:S(2)}) %all-to-all-start.1) | async-done | bytes 131104 | tf_op jit(solution)/shard_map/all_to_all | solution.py:309
  79.2 0.0 copy-done
  79.2 0.2 mix.1
  79.4 13.1 %all_to_all.15.got = bf16[8,32,256]{2,1,0:T(8,128)(2,1)S(1)} all-to-all(bf16[8,32,256]{2,1,0:T(8,128)(2,1)S(1)} %mix.1), channel_id=1, replica_groups=mesh['grp'=2,'kv'=16,'tp'=8] {'tp'}, dimensions={0} | all-to-all | bytes 262144 | tf_op jit(solution)/shard_map/all_to_all | solution.py:344
  92.5 0.8 finish.1
  (4 shorter events, 0.0 us)
Async XLA Ops:
  0.6 31.9 %copy-start.1 = (s32[4]{0:T(128)S(1)}, s32[4]{0:T(128)}, u32[]{:S(2)}) copy-start(s32[4]{0:T(128)} %accepted.3) | copy-start | bytes 52
  3.7 48.4 %all-to-all-start = ((bf16[16,136,128]{2,1,0:T(8,128)(2,1)}), bf16[16,136,128]{2,1,0:T(8,128)(2,1)S(1)}, u32[]{:S(2)}, u32[]{:S(2)}) async-start(bf16[16,136,128]{2,1,0:T(8,128)(2,1)} %project.1), calls=%async_computation | async-start | bytes 1114112 | tf_op jit(solution)/shard_map/all_to_all | solution.py:291
  32.5 46.7 %copy-start = (bf16[256,256]{1,0:T(8,128)(2,1)S(1)}, bf16[256,256]{1,0:T(8,128)(2,1)}, u32[]{:S(2)}) copy-start(bf16[256,256]{1,0:T(8,128)(2,1)} %w.1) | copy-start | bytes 393220
  54.4 24.8 %all-to-all-start.1 = ((bf16[16,16,256]{2,1,0:T(8,128)(2,1)}), bf16[16,16,256]{2,1,0:T(8,128)(2,1)S(1)}, u32[]{:S(2)}, u32[]{:S(2)}) async-start(bf16[16,16,256]{2,1,0:T(8,128)(2,1)} %get-tuple-element.10), calls=%async_computation.1 | async-start | bytes 262144 | tf_op jit(solution)/shard_map/all_to_all | solution.py:309

commit v3 on v2

--- a/solution.py
+++ b/solution.py
@@ -32,7 +32,7 @@
     return jnp.where(y < 0.0, -root, root)
 
 
-def project_kernel(tokens, gain, wq, wk, wv, wo, gates_hbm, out, gates, sem, *, owners):
+def project_kernel(tokens, gain, wq, wk, wv, wo, gates_hbm, up, down, keep_up, keep_down, small, gates, sem, *, owners):
     z, tp = lax.axis_index("kv"), lax.axis_index("tp")
     seqs, props, width = tokens.shape
     fetch = pltpu.make_async_copy(gates_hbm.at[:, :, pl.ds(pl.multiple_of(z * width, width), width)], gates, sem)
@@ -51,12 +51,18 @@
     source = (r & -per) + (r & (own - 1)) * props + ((r & (per - 1)) >> log2(own))
     move = jnp.where(c == source, 1.0, 0.0).astype(BF16)
     scaled = contract(move, scaled, 1, 0).astype(BF16)
-    block = 0
-    for w in (wq, wk, wv, wo):
-        y = coded(contract(scaled, w[...], 1, 0))
-        for h in range(y.shape[1] // 128):
-            out[:, block * per : (block + 1) * per, :] = y[:, h * 128 : (h + 1) * 128].reshape(owners, per, 128)
-            block += 1
+    even = (z & 1) == 0
+
+    def blocked(y):
+        return [y[:, h * 128 : (h + 1) * 128].reshape(owners, per, 128) for h in range(y.shape[1] // 128)]
+
+    for first, second, given, kept in ((wq, wk, up, keep_up), (wv, wo, down, keep_down)):
+        theirs = jnp.where(even, second[...], first[...])
+        ours = jnp.where(even, first[...], second[...])
+        for h, y in enumerate(blocked(coded(contract(scaled, theirs, 1, 0)))):
+            given[:, h * per : (h + 1) * per, :] = y
+        for h, y in enumerate(blocked(contract(scaled, ours, 1, 0))):
+            kept[:, h * per : (h + 1) * per, :] = y
     square = x * x
     s_hi = square.astype(BF16)
     s_lo = (square - s_hi.astype(F32)).astype(BF16)
@@ -85,7 +91,14 @@
         low = jnp.where(lanes < 64, gh, sh).astype(BF16)
         high = jnp.where(lanes < 64, sh, gh).astype(BF16)
         for k in range(span):
-            out[half * span + k, block * per :, :] = low if k < span // 2 else high
+            small[half * span + k] = low if k < span // 2 else high
+
+
+def merge_kernel(got_up, got_down, keep_up, keep_down, small, out):
+    half = got_up.shape[1]
+    for at, got, kept in ((0, got_up, keep_up), (half, got_down, keep_down)):
+        out[:, at : at + half, :] = coded(kept[...] + decoded(got[...]) * (1.0 / SHIFT))
+    out[:, 2 * half :, :] = small[...]
 
 
 def cell_kernel(accepted, stab, ib, fb, got, m0, n0, gated, kv_out, coef, *, features):
@@ -93,7 +106,7 @@
     owners = got.shape[0]
     own, _, heads, dim, _ = m0.shape
     main = got.shape[1] - 8
-    per = main // (4 * heads)
+    per = main // (2 * heads)
     props = per // own
     small = got[0, main:].astype(F32)
     for k in range(1, owners):
@@ -131,10 +144,10 @@
     rr = iota((per, dim), 0) & (own - 1)
 
     def part(kind, h):
-        rows = slice((kind * heads + h) * per, (kind * heads + h + 1) * per)
-        total = decoded(got[0, rows])
-        for k in range(1, owners):
-            total = total + decoded(got[k, rows])
+        at = ((kind >> 1) * heads + h) * per
+        total = decoded(got[kind & 1, at : at + per])
+        for k in range(2 + (kind & 1), owners, 2):
+            total = total + decoded(got[k, at : at + per])
         return (total * factor).astype(BF16)
 
     outs = []
@@ -272,21 +285,39 @@
     own, saved, _, dim, _ = saved_memory.shape
     columns = w_query.shape[1]
     per = own * props
-    blocks = 4 * columns // 128
     gates = gate_weight.transpose(0, 2, 1)
     all_heads = gates.shape[1]
 
     def whole(shape):
         return pl.BlockSpec(shape, lambda *_: (0,) * len(shape))
 
-    send = pl.pallas_call(
+    half = columns // 128 * per
+    up, down, keep_up, keep_down, small = pl.pallas_call(
         functools.partial(project_kernel, owners=owners),
         in_specs=[VMEM] * 6 + [pl.BlockSpec(memory_space=pl.ANY)],
-        out_specs=[VMEM],
-        out_shape=[held((owners, blocks * per + 8, 128), BF16)],
+        out_specs=[VMEM] * 5,
+        out_shape=[
+            held((owners, half, 128), BF16),
+            held((owners, half, 128), BF16),
+            held((owners, half, 128), F32),
+            held((owners, half, 128), F32),
+            held((owners, 8, 128), BF16),
+        ],
         scratch_shapes=[pltpu.VMEM((2, all_heads, width), BF16), pltpu.SemaphoreType.DMA],
         name="project",
-    )(tokens, norm_gain.reshape(-1, 128), w_query, w_key, w_value, w_outgate, gates)[0]
+    )(tokens, norm_gain.reshape(-1, 128), w_query, w_key, w_value, w_outgate, gates)
+
+    with_next = [(i, i ^ 1) for i in range(owners)]
+    with_last = [(i, (((i + 1) ^ 1) - 1) % owners) for i in range(owners)]
+    got_up = lax.ppermute(up, "kv", with_next)
+    got_down = lax.ppermute(down, "kv", with_last)
+    send = pl.pallas_call(
+        merge_kernel,
+        in_specs=[VMEM] * 5,
+        out_specs=[VMEM],
+        out_shape=[held((owners, 2 * half + 8, 128), BF16)],
+        name="merge",
+    )(near(got_up), near(got_down), near(keep_up), near(keep_down), near(small))[0]
 
     got = lax.all_to_all(send, "kv", split_axis=0, concat_axis=0, tiled=True)
 

time: 94 us -> 88.7 us (0.944)
  waiting for transfers between devices: 26.2 us -> 19.1 us
  starting transfers between devices: 37.6 us -> 39.4 us
    ppermute x0 -> x2, starting transfers between devices: none -> 23.2 us  [the longest x1 19.7 us: local(): got_down = lax.ppermute(down, 'kv', with_last)]
    all_to_all x1, starting transfers between devices: 24.5 us -> 4 us  [local(): got = lax.all_to_all(send, 'kv', split_axis=0, concat_axis=0, tiled=True)]
    all_to_all x1, waiting for transfers between devices: 19.3 us -> 8.98 us  [local(): got = lax.all_to_all(send, 'kv', split_axis=0, concat_axis=0, tiled=True)]
    ppermute x0 -> x2, waiting for transfers between devices: none -> 3.28 us  [the longest x1 3.28 us: local(): got_down = lax.ppermute(down, 'kv', with_last)]
    pallas_call x0 -> x1, Pallas kernels: none -> 0.99 us  [local(): pl.pallas_call(merge_kernel, in_specs=[VMEM] * 5, out_specs=[VMEM], out_s...]
  transfers between devices with their start and end apart: 2 -> 4, of which waited for: 2 -> 3; matrix products, arithmetic and copies ran while one was open for 5% -> 4% of each run, Pallas kernels for 5% -> 6%
where the time goes in v3:
time: 88.7 us; the launch traced here: 88.1 us
  starting transfers between devices  39.4 us (44%)
  waiting for transfers between devices  19.1 us (22%)
  blocking collectives  13.3 us (15%)
  Pallas kernels  11.7 us (13%)
  local copies, waits for them, and re-layouts  3.64 us (4%)
    ppermute x1, starting transfers between devices, local(): got_down = lax.ppermute(down, 'kv', with_last)  19.7 us
    all_to_all x1, blocking collectives, local(): lax.all_to_all(terms, 'tp', split_axis=0, concat_axis=0, tiled=True)  13.3 us
    all_to_all x1, starting transfers between devices, local(): lax.all_to_all(gated, 'kv', split_axis=0, concat_axis=0, tiled=True)  12.2 us
    all_to_all x1, waiting for transfers between devices, local(): got = lax.all_to_all(send, 'kv', split_axis=0, concat_axis=0, tiled=True)  8.98 us
    all_to_all x1, waiting for transfers between devices, local(): lax.all_to_all(gated, 'kv', split_axis=0, concat_axis=0, tiled=True)  6.85 us
    pallas_call x1, Pallas kernels, local(): pl.pallas_call(functools.partial(memory_kernel, heads=heads), grid_spec=p...  4.9 us
    all_to_all x1, starting transfers between devices, local(): got = lax.all_to_all(send, 'kv', split_axis=0, concat_axis=0, tiled=True)  4 us
    ppermute x1, starting transfers between devices, local(): got_up = lax.ppermute(up, 'kv', with_next)  3.45 us
  transfers between devices with their start and end apart: 4, of which 3 were waited for; matrix products, arithmetic and copies ran while one was open for 4% of the time, Pallas kernels for 6%

profile of v3, /device:TPU:33, one launch (start us, length us, event | category | flops | bytes accessed | tf_op | source)
XLA Modules:
  0.0 88.1 jit_solution(3886465342503300263)
XLA Ops:
  0.6 0.0 copy-start.1
  0.6 2.6 %project.1 = (bf16[16,32,128]{2,1,0:T(8,128)(2,1)S(1)}, bf16[16,32,128]{2,1,0:T(8,128)(2,1)S(1)}, f32[16,32,128]{2,1,0:T(8,128)S(1)}, f32[16,32,128]{2,1,0:T(8,128)S(1)}, bf16[16,8,128]{2,1,0:T(8,128)(2,1)S(1)}) custom-call(bf16[64,4,256]{2,1,0:T(4,128)(2,1)} %tokens.1, bf16[32,128]{1,0:T(8,128)(2,1)} %bitcast.15, bf16[256,256]{1,0:T(8,128)(2,1)} %wq.1, ...), custom_call_target="tpu_custom_call" | custom-call | tf_op jit(solution)/shard_map/project/pallas_call | solution.py:295
  3.3 3.5 %collective-permute-start = (bf16[16,32,128]{2,1,0:T(8,128)(2,1)S(1)}, bf16[16,32,128]{2,1,0:T(8,128)(2,1)S(1)}, u32[]{:S(2)}, u32[]{:S(2)}) collective-permute-start(bf16[16,32,128]{2,1,0:T(8,128)(2,1)S(1)} %get-tuple-element.15), channel_id=1, source_target_pairs={{0,8},{8,0},{16,24},{24,16},{32,40},{40,32},{48,56},{56,48},{64,72... | collective-permute-start | bytes 393224 | tf_op jit(solution)/shard_map/ppermute | solution.py:312
  6.7 19.7 %collective-permute-start.1 = (bf16[16,32,128]{2,1,0:T(8,128)(2,1)S(1)}, bf16[16,32,128]{2,1,0:T(8,128)(2,1)S(1)}, u32[]{:S(2)}, u32[]{:S(2)}) collective-permute-start(bf16[16,32,128]{2,1,0:T(8,128)(2,1)S(1)} %get-tuple-element.16), channel_id=1, source_target_pairs={{0,120},{8,16},{16,8},{24,32},{32,24},{40,48},{48,40},{56,64},{64,... | collective-permute-start | bytes 393224 | tf_op jit(solution)/shard_map/ppermute | solution.py:313
  26.5 0.0 collective-permute-done.got_up
  26.5 3.3 %collective-permute-done.1.got_down = bf16[16,32,128]{2,1,0:T(8,128)(2,1)S(1)} collective-permute-done((bf16[16,32,128]{2,1,0:T(8,128)(2,1)S(1)}, bf16[16,32,128]{2,1,0:T(8,128)(2,1)S(1)}, u32[]{:S(2)}, u32[]{:S(2)}) %collective-permute-start.1) | collective-permute-done | bytes 131104 | tf_op jit(solution)/shard_map/ppermute | solution.py:313
  29.8 1.0 %merge.1 = bf16[16,72,128]{2,1,0:T(8,128)(2,1)} custom-call(bf16[16,32,128]{2,1,0:T(8,128)(2,1)S(1)} %collective-permute-done.got_up, bf16[16,32,128]{2,1,0:T(8,128)(2,1)S(1)} %collective-permute-done.1.got_down, f32[16,32,128]{2,1,0:T(8,128)S(1)} %get-tuple-element.17.keep_up, f32[16,32,128]{2,1,0:T(8,128)S(1)} %get-tuple-element.18.keep_down, ...), custom_call_target="tpu_custom_call" | custom-call | tf_op jit(solution)/shard_map/merge/pallas_call | solution.py:314
  30.8 4.0 %all-to-all-start = ((bf16[16,72,128]{2,1,0:T(8,128)(2,1)}), bf16[16,72,128]{2,1,0:T(8,128)(2,1)S(1)}, u32[]{:S(2)}, u32[]{:S(2)}) async-start(bf16[16,72,128]{2,1,0:T(8,128)(2,1)} %merge.1), calls=%async_computation | async-start | bytes 589824 | tf_op jit(solution)/shard_map/all_to_all | solution.py:322
  34.8 0.0 copy-done.1
  34.8 1.3 %gather_fusion.1 = f32[4,2,128]{2,1,0:T(2,128)S(1)} fusion(f32[4,5,2,128]{3,2,1,0:T(2,128)} %n0.1, s32[4]{0:T(128)S(1)} %or_bitcast_fusion), kind=kCustom, calls=%fused_computation.1 | custom fusion | bytes 8224 | tf_op jit(solution)/shard_map/jit(take_along_axis)/gather | solution.py:324
  36.1 2.3 %gather_fusion = f32[4,2,128,128]{3,2,1,0:T(8,128)S(1)} fusion(f32[4,5,2,128,128]{4,3,2,1,0:T(8,128)} %m0.1, s32[4]{0:T(128)S(1)} %or_bitcast_fusion), kind=kCustom, calls=%fused_computation | custom fusion | bytes 1048608 | tf_op jit(solution)/shard_map/jit(take_along_axis)/gather | solution.py:325
  38.5 0.0 copy-start
  38.5 0.1 broadcast_select_fusion.n0
  38.6 0.1 bitcast_select_fusion.m0
  38.7 9.0 %all-to-all-done.got = bf16[16,72,128]{2,1,0:T(8,128)(2,1)S(1)} async-done(((bf16[16,72,128]{2,1,0:T(8,128)(2,1)}), bf16[16,72,128]{2,1,0:T(8,128)(2,1)S(1)}, u32[]{:S(2)}, u32[]{:S(2)}) %all-to-all-start) | async-done | bytes 294944 | tf_op jit(solution)/shard_map/all_to_all | solution.py:322
  47.7 2.1 %cell.1 = (bf16[16,16,256]{2,1,0:T(8,128)(2,1)}, bf16[4,16,128]{2,1,0:T(8,128)(2,1)S(1)}, f32[5,4,6]{2,1,0:T(4,128)}) custom-call(s32[4]{0:T(128)} %accepted.3, f32[4,2,5]{2,1,0:T(2,128)} %bitcast.16, f32[2]{0:T(128)} %ib.1, f32[2]{0:T(128)} %fb.1, bf16[16,72,128]{2,1,0:T(8,128)(2,1)S(1)} %all-to-all-done.got, ...), custom_call_target="tpu_custom_call" | custom-call | tf_op jit(solution)/shard_map/cell/pallas_call | solution.py:328
  49.8 12.2 %all-to-all-start.1 = ((bf16[16,16,256]{2,1,0:T(8,128)(2,1)}), bf16[16,16,256]{2,1,0:T(8,128)(2,1)S(1)}, u32[]{:S(2)}, u32[]{:S(2)}) async-start(bf16[16,16,256]{2,1,0:T(8,128)(2,1)} %get-tuple-element.20), calls=%async_computation.1 | async-start | bytes 262144 | tf_op jit(solution)/shard_map/all_to_all | solution.py:340
  62.0 4.9 %memory.1 = (f32[4,5,2,128,128]{4,3,2,1,0:T(8,128)}, f32[4,5,2,128]{3,2,1,0:T(2,128)}, f32[4,2,5]{2,1,0:T(2,128)}) custom-call(s32[4]{0:T(128)} %accepted.3, f32[5,4,6]{2,1,0:T(4,128)} %get-tuple-element.21.coef, f32[4,5,2,128,128]{4,3,2,1,0:T(8,128)} %m0.1, f32[4,5,2,128]{3,2,1,0:T(2,128)} %n0.1, bf16[4,16,128]{2,1,0:T(8,128)(2,1)S(1)} %get-tuple-element.22.kv), custom_call_target="tpu_custom_call" | custom-call | flops 20000000 | bytes 3200000 | tf_op jit(solution)/shard_map/memory/pallas_call | solution.py:342
  66.9 6.9 %all-to-all-done.1.gathered = bf16[16,16,256]{2,1,0:T(8,128)(2,1)S(1)} async-done(((bf16[16,16,256]{2,1,0:T(8,128)(2,1)}), bf16[16,16,256]{2,1,0:T(8,128)(2,1)S(1)}, u32[]{:S(2)}, u32[]{:S(2)}) %all-to-all-start.1) | async-done | bytes 131104 | tf_op jit(solution)/shard_map/all_to_all | solution.py:340
  73.7 0.0 copy-done
  73.7 0.2 mix.1
  74.0 13.3 %all_to_all.15.got = bf16[8,32,256]{2,1,0:T(8,128)(2,1)S(1)} all-to-all(bf16[8,32,256]{2,1,0:T(8,128)(2,1)S(1)} %mix.1), channel_id=1, replica_groups=mesh['grp'=2,'kv'=16,'tp'=8] {'tp'}, dimensions={0} | all-to-all | bytes 262144 | tf_op jit(solution)/shard_map/all_to_all | solution.py:375
  87.2 0.8 finish.1
  (5 shorter events, 0.0 us)
Async XLA Ops:
  0.6 34.1 %copy-start.1 = (s32[4]{0:T(128)S(1)}, s32[4]{0:T(128)}, u32[]{:S(2)}) copy-start(s32[4]{0:T(128)} %accepted.3) | copy-start | bytes 52
  3.3 23.2 %collective-permute-start = (bf16[16,32,128]{2,1,0:T(8,128)(2,1)S(1)}, bf16[16,32,128]{2,1,0:T(8,128)(2,1)S(1)}, u32[]{:S(2)}, u32[]{:S(2)}) collective-permute-start(bf16[16,32,128]{2,1,0:T(8,128)(2,1)S(1)} %get-tuple-element.15), channel_id=1, source_target_pairs={{0,8},{8,0},{16,24},{24,16},{32,40},{40,32},{48,56},{56,48},{64,72... | collective-permute-start | bytes 393224 | tf_op jit(solution)/shard_map/ppermute | solution.py:312
  6.7 23.0 %collective-permute-start.1 = (bf16[16,32,128]{2,1,0:T(8,128)(2,1)S(1)}, bf16[16,32,128]{2,1,0:T(8,128)(2,1)S(1)}, u32[]{:S(2)}, u32[]{:S(2)}) collective-permute-start(bf16[16,32,128]{2,1,0:T(8,128)(2,1)S(1)} %get-tuple-element.16), channel_id=1, source_target_pairs={{0,120},{8,16},{16,8},{24,32},{32,24},{40,48},{48,40},{56,64},{64,... | collective-permute-start | bytes 393224 | tf_op jit(solution)/shard_map/ppermute | solution.py:313
  30.8 16.9 %all-to-all-start = ((bf16[16,72,128]{2,1,0:T(8,128)(2,1)}), bf16[16,72,128]{2,1,0:T(8,128)(2,1)S(1)}, u32[]{:S(2)}, u32[]{:S(2)}) async-start(bf16[16,72,128]{2,1,0:T(8,128)(2,1)} %merge.1), calls=%async_computation | async-start | bytes 589824 | tf_op jit(solution)/shard_map/all_to_all | solution.py:322
  38.5 35.3 %copy-start = (bf16[256,256]{1,0:T(8,128)(2,1)S(1)}, bf16[256,256]{1,0:T(8,128)(2,1)}, u32[]{:S(2)}) copy-start(bf16[256,256]{1,0:T(8,128)(2,1)} %w.1) | copy-start | bytes 393220
  49.8 23.9 %all-to-all-start.1 = ((bf16[16,16,256]{2,1,0:T(8,128)(2,1)}), bf16[16,16,256]{2,1,0:T(8,128)(2,1)S(1)}, u32[]{:S(2)}, u32[]{:S(2)}) async-start(bf16[16,16,256]{2,1,0:T(8,128)(2,1)} %get-tuple-element.20), calls=%async_computation.1 | async-start | bytes 262144 | tf_op jit(solution)/shard_map/all_to_all | solution.py:340

commit v4 on v3

v4 whole, which is shorter than its diff:
```python
import functools

import jax
import jax.numpy as jnp
from jax import lax
from jax.experimental import pallas as pl
from jax.experimental.pallas import tpu as pltpu
from jax.sharding import PartitionSpec as P

EPSILON = 1e-06
F32 = jnp.float32
BF16 = jnp.bfloat16
SHIFT = 2.0**20
TURN = ((1, 1, 0), (1, 1, 8))


def iota(shape, dim):
    return lax.broadcasted_iota(jnp.int32, shape, dim)


def contract(a, b, da, db):
    return lax.dot_general(a, b, (((da,), (db,)), ((), ())), preferred_element_type=F32)


def coded(x):
    y = x * SHIFT
    return ((y * jnp.abs(y)) * (y * y)).astype(BF16)


def decoded(y):
    y = y.astype(F32)
    root = lax.rsqrt(lax.rsqrt(jnp.maximum(jnp.abs(y), 1e-37)))
    return jnp.where(y < 0.0, -root, root)


def moved_rows(rows, per, own):
    r, c = iota((rows, rows), 0), iota((rows, rows), 1)
    stride, _, start = TURN[0]
    place = ((r & -per) * stride + start * per) & (rows - 1)
    source = place + (r & (own - 1)) * (per // own) + ((r & (per - 1)) >> log2(own))
    return jnp.where(c == source, 1.0, 0.0).astype(BF16)


def blocked(y, owners):
    return [y[:, h * 128 : (h + 1) * 128].reshape(owners, -1, 128) for h in range(y.shape[1] // 128)]


def give_kernel(tokens, gain, wq, wk, wv, wo, up, down, scaled_out, *, owners):
    z = lax.axis_index("kv")
    seqs, props, width = tokens.shape
    rows = seqs * props
    per = rows // owners
    own = per // props
    x = tokens[...].astype(F32).reshape(rows, width)
    gain_rows = gain[...].astype(F32)
    pieces = []
    for j in range(width // 128):
        hit = iota(gain_rows.shape, 0) == z * (width // 128) + j
        pieces.append(jnp.sum(jnp.where(hit, gain_rows, 0.0), 0, keepdims=True))
    scaled = (x * jnp.concatenate(pieces, 1)).astype(BF16)
    scaled = contract(moved_rows(rows, per, own), scaled, 1, 0).astype(BF16)
    scaled_out[...] = scaled
    even = (z & 1) == 0
    for first, second, given in ((wq, wk, up), (wv, wo, down)):
        theirs = jnp.where(even, second[...], first[...])
        for h, y in enumerate(blocked(coded(contract(scaled, theirs, 1, 0)), owners)):
            given[:, h * per : (h + 1) * per, :] = y


def keep_kernel(tokens, scaled_in, wq, wk, wv, wo, gates_hbm, keep_up, keep_down, small, gates, sem, *, owners):
    z, tp = lax.axis_index("kv"), lax.axis_index("tp")
    seqs, props, width = tokens.shape
    fetch = pltpu.make_async_copy(gates_hbm.at[:, :, pl.ds(pl.multiple_of(z * width, width), width)], gates, sem)
    fetch.start()
    rows = seqs * props
    per = rows // owners
    own = per // props
    x = tokens[...].astype(F32).reshape(rows, width)
    scaled = scaled_in[...]
    even = (z & 1) == 0
    for first, second, kept in ((wq, wk, keep_up), (wv, wo, keep_down)):
        ours = jnp.where(even, first[...], second[...])
        for h, y in enumerate(blocked(contract(scaled, ours, 1, 0), owners)):
            kept[:, h * per : (h + 1) * per, :] = y
    move = moved_rows(rows, per, own)
    square = x * x
    s_hi = square.astype(BF16)
    s_lo = (square - s_hi.astype(F32)).astype(BF16)
    ones = jnp.ones((8, width), BF16)
    s = contract(ones, contract(move, s_hi, 1, 0).astype(BF16), 1, 1)
    s += contract(ones, contract(move, s_lo, 1, 0).astype(BF16), 1, 1)
    fetch.wait()
    heads = gates.shape[1]
    local = heads // lax.axis_size("tp")
    pick_r, pick_c = iota((8, 2 * heads), 0), iota((8, 2 * heads), 1)
    want = ((pick_r & 3) // local) * heads + tp * local + (pick_r & (local - 1))
    pick = jnp.where(pick_c == want, 1.0, 0.0).astype(BF16)
    own_gates = contract(pick, gates[...].reshape(2 * heads, width), 1, 0).astype(BF16)
    g = contract(own_gates, scaled, 1, 1)

    def words(value, split):
        hi = value.astype(BF16).astype(F32)
        return jnp.where(iota(value.shape, 0) < split, hi, value - hi)

    g, s = words(g, 4), words(s, 1)
    lanes = iota((8, 128), 1)
    span = 128 // per
    for half in range(rows // 128):
        gh = g[:, half * 128 : (half + 1) * 128]
        sh = pltpu.roll(s[:, half * 128 : (half + 1) * 128], 64, 1)
        low = jnp.where(lanes < 64, gh, sh).astype(BF16)
        high = jnp.where(lanes < 64, sh, gh).astype(BF16)
        for k in range(span):
            small[half * span + k] = low if k < span // 2 else high


def merge_kernel(got_up, got_down, keep_up, keep_down, small, out, made, sems):
    owners, half, _ = got_up.shape
    quarter = owners // 4
    copies = []
    for part in range(4):
        own = slice(part * quarter, (part + 1) * quarter)
        for at, got, kept in ((0, got_up, keep_up), (half, got_down, keep_down)):
            made[own, at : at + half, :] = coded(kept[own] + decoded(got[own]) * (1.0 / SHIFT))
        made[own, 2 * half :, :] = small[own]
        copies.append(pltpu.make_async_copy(made.at[own], out.at[own], sems.at[part]))
        copies[part].start()
    for copy in copies:
        copy.wait()


def take_kernel(accepted, stab, ib, fb, memory_hbm, norms, m0, n0, words, move, bias, first, sems, *, owners, seqs):
    own, _, heads, dim, _ = m0.shape
    copies = []
    for b in range(own):
        copies.append(pltpu.make_async_copy(memory_hbm.at[b, accepted[b]], m0.at[b, 0], sems.at[b]))
        copies[b].start()
    col = iota(bias.shape[1:], 1)
    for k, source in enumerate((ib, fb)):
        value = jnp.zeros(bias.shape[1:], F32)
        for h in range(heads):
            value = jnp.where(col == h, source[h], value)
        bias[k] = value
    srow, scol = iota((own, heads), 0), iota((own, heads), 1)
    m = jnp.zeros((own, heads), F32)
    for b in range(own):
        for h in range(heads):
            m = jnp.where((srow == b) & (scol == h), stab[b, h, accepted[b]], m)
    first[...] = m
    rows = move.shape[0]
    props = rows // seqs
    per = rows // owners
    r, c = iota((rows, rows), 0), iota((rows, rows), 1)
    t, rest = c >> log2(seqs), c & (seqs - 1)
    place = (((rest >> log2(own)) - TURN[1][2]) * TURN[1][1]) & (owners - 1)
    source = place * per + t * own + (rest & (own - 1))
    move[...] = jnp.where(r == source, 1.0, 0.0).astype(BF16)
    for b in range(own):
        n0[b] = norms[b, accepted[b]]
        copies[b].wait()
        for h in range(heads):
            value = m0[b, 0, h]
            hi = value.astype(BF16)
            words[h, b * dim : (b + 1) * dim, :dim] = hi
            words[h, b * dim : (b + 1) * dim, dim:] = (value - hi.astype(F32)).astype(BF16)


def cell_kernel(got, words, n0, bias, start, gated, kv_out, coef, *, features):
    z = lax.axis_index("kv")
    owners = got.shape[0]
    own, heads, dim = n0.shape
    main = got.shape[1] - 8
    per = main // (2 * heads)
    props = per // own
    small = got[0, main:].astype(F32)
    for k in range(1, owners):
        small = small + got[k, main:].astype(F32)
    shift = (((z - TURN[0][2]) * TURN[0][1]) & (128 // per - 1)) * per
    small = pltpu.roll(small, (128 - shift) & 127, 1)
    g = small + pltpu.roll(small, 4, 0)
    sq = pltpu.roll(small + pltpu.roll(small, 7, 0), 64, 1)
    packed = jnp.where(iota(g.shape, 0) < 4, g, pltpu.roll(sq, 4, 0))
    cols = packed.T[:per]
    inverse = lax.rsqrt(cols[:, 4:5] / features + EPSILON)
    in_gate = cols[:, 0:2] * inverse + bias[0]
    f = cols[:, 2:4] * inverse + bias[1]
    log_forget = jnp.minimum(f, 0.0) - jnp.log1p(jnp.exp(-jnp.abs(f)))
    m = start[...]
    stabs, retain, admit = [m], [], []
    for t in range(props):
        carried = log_forget[t * own : (t + 1) * own] + m
        incoming = in_gate[t * own : (t + 1) * own]
        top = jnp.maximum(carried, incoming)
        retain.append(jnp.exp(carried - top))
        admit.append(jnp.exp(incoming - top))
        m = top
        stabs.append(m)
    scale = dim ** (-0.5)
    factor = inverse * (1.0 / SHIFT)
    rr = iota((per, dim), 0) & (own - 1)

    def part(kind, h):
        at = ((kind >> 1) * heads + h) * per
        first = (kind + TURN[0][2]) & 1
        total = decoded(got[first, at : at + per])
        for k in range(2 + first, owners, 2):
            total = total + decoded(got[k, at : at + per])
        return (total * factor).astype(BF16)

    outs = []
    for h in range(heads):
        q, k, v, o = part(0, h), part(1, h), part(2, h), part(3, h)
        kv_out[h] = k
        kv_out[heads + h] = v
        qf, kf, vf = q.astype(F32), k.astype(F32) * scale, v.astype(F32)
        wide = jnp.concatenate([jnp.where(rr == b, qf, 0.0) for b in range(own)], 1).astype(BF16)
        both = contract(wide, words[h], 1, 0)
        base = both[:, :dim] + both[:, dim:]
        norm = n0[:, h, :]
        rows = []
        for t in range(props):
            sl = slice(t * own, (t + 1) * own)
            norm = retain[t][:, h : h + 1] * norm + admit[t][:, h : h + 1] * kf[sl]
            den = jnp.sum(qf[sl] * norm, -1, keepdims=True)
            weight = jnp.ones((own, 1), F32)
            num = jnp.zeros((own, dim), F32)
            for s in range(t, -1, -1):
                ss = slice(s * own, (s + 1) * own)
                dots = jnp.sum(qf[sl] * kf[ss], -1, keepdims=True)
                num += (weight * admit[s][:, h : h + 1] * dots) * vf[ss]
                weight = weight * retain[s][:, h : h + 1]
            num += weight * base[sl]
            floor = jnp.exp(-stabs[t + 1][:, h : h + 1])
            rows.append(num / jnp.maximum(jnp.abs(den), floor))
        hidden = jnp.concatenate(rows, 0)
        outs.append(jax.nn.sigmoid(o.astype(F32)) * hidden)
    result = jnp.concatenate(outs, 1).astype(BF16)
    for k in range(gated.shape[0]):
        gated[k] = result
    for t in range(props + 1):
        last = t - 1 if t else 0
        coef[t] = jnp.concatenate([stabs[t], retain[last], admit[last]], 1)


def memory_kernel(coef, m0, n0, kv, new_m, new_n, new_s, made, sems):
    own, _, heads, dim, _ = m0.shape
    per = kv.shape[1]
    props = per // own
    steps = props + 1
    scale = dim ** (-0.5)
    row, col = iota((heads, steps), 0), iota((heads, steps), 1)
    row_at = iota((per, dim), 0)
    sent = []

    def send(source, b, t):
        copy = pltpu.make_async_copy(source, new_m.at[b, t], sems.at[b, t])
        copy.start()
        sent.append(copy)

    for b in range(own):
        send(m0.at[b, 0], b, 0)
    for b in range(own):
        stabs = jnp.zeros((heads, steps), F32)
        norms = []
        for h in range(heads):
            norms.append(n0[b, h : h + 1])
            new_n[b, 0, h : h + 1] = norms[h]
            for t in range(steps):
                stabs = jnp.where((row == h) & (col == t), coef[t, b, h], stabs)
        new_s[b] = stabs
        memories = [m0[b, 0, h] for h in range(heads)]
        for t in range(props):
            for h in range(heads):
                keep, add = coef[t + 1, b, heads + h], coef[t + 1, b, 2 * heads + h] * scale
                one = jnp.where(row_at == t * own + b, kv[h].astype(F32), 0.0)
                memories[h] = keep * memories[h] + add * contract(one.astype(BF16), kv[heads + h], 0, 0)
                norms[h] = keep * norms[h] + add * jnp.sum(one, 0, keepdims=True)
                made[b, t, h] = memories[h]
                new_n[b, t + 1, h : h + 1] = norms[h]
            send(made.at[b, t], b, t + 1)
    for copy in sent:
        copy.wait()


def mix_kernel(gathered, w, after, out):
    owners, per, _ = gathered.shape
    rows = owners * per
    y = contract(w[...], gathered[...].reshape(rows, gathered.shape[2]), 0, 1).astype(BF16)
    out[...] = y.reshape(out.shape)


def finish_kernel(got, move, out):
    total = got[0].astype(F32)
    for k in range(1, got.shape[0]):
        total = total + got[k].astype(F32)
    props, _, seqs = out.shape
    y = contract(total.astype(BF16), move[...], 1, 0).astype(BF16)
    for t in range(props):
        out[t] = y[:, t * seqs : (t + 1) * seqs]


def log2(n):
    assert n & (n - 1) == 0
    return n.bit_length() - 1


SMEM = pl.BlockSpec(memory_space=pltpu.SMEM)
VMEM = pl.BlockSpec(memory_space=pltpu.VMEM)


def held(shape, dtype):
    return pltpu.VMEM(shape, dtype)


def near(x):
    return pltpu.with_memory_space_constraint(x, pltpu.VMEM)


def local(
    tokens,
    norm_gain,
    w_query,
    w_key,
    w_value,
    w_outgate,
    gate_weight,
    input_bias,
    forget_bias,
    w_out,
    saved_memory,
    saved_normalizer,
    saved_stabilizer,
    accepted,
):
    owners, peers = lax.axis_size("kv"), lax.axis_size("tp")
    seqs, props, width = tokens.shape
    heads = input_bias.shape[0]
    own, saved, _, dim, _ = saved_memory.shape
    columns = w_query.shape[1]
    per = own * props
    gates = gate_weight.transpose(0, 2, 1)
    all_heads = gates.shape[1]

    def whole(shape):
        return pl.BlockSpec(shape, lambda *_: (0,) * len(shape))

    half = columns // 128 * per
    weights = (w_query, w_key, w_value, w_outgate)
    up, down, scaled = pl.pallas_call(
        functools.partial(give_kernel, owners=owners),
        in_specs=[VMEM] * 6,
        out_specs=[VMEM] * 3,
        out_shape=[
            held((owners, half, 128), BF16),
            held((owners, half, 128), BF16),
            held((seqs * props, width), BF16),
        ],
        name="give",
    )(tokens, norm_gain.reshape(-1, 128), *weights)

    with_next = [(i, i ^ 1) for i in range(owners)]
    with_last = [(i, (((i + 1) ^ 1) - 1) % owners) for i in range(owners)]
    got_up = lax.ppermute(up, "kv", with_next)
    got_down = lax.ppermute(down, "kv", with_last)
    keep_up, keep_down, small = pl.pallas_call(
        functools.partial(keep_kernel, owners=owners),
        in_specs=[VMEM] * 6 + [pl.BlockSpec(memory_space=pl.ANY)],
        out_specs=[VMEM] * 3,
        out_shape=[
            held((owners, half, 128), F32),
            held((owners, half, 128), F32),
            held((owners, 8, 128), BF16),
        ],
        scratch_shapes=[pltpu.VMEM((2, all_heads, width), BF16), pltpu.SemaphoreType.DMA],
        cost_estimate=pl.CostEstimate(flops=80_000_000, bytes_accessed=1_000_000, transcendentals=0),
        name="keep",
    )(tokens, near(scaled), *weights, gates)
    send = pl.pallas_call(
        merge_kernel,
        in_specs=[VMEM] * 5,
        out_specs=[pl.BlockSpec(memory_space=pl.ANY)],
        out_shape=[jax.ShapeDtypeStruct((owners, 2 * half + 8, 128), BF16)],
        scratch_shapes=[pltpu.VMEM((owners, 2 * half + 8, 128), BF16), pltpu.SemaphoreType.DMA((4,))],
        name="merge",
    )(near(got_up), near(got_down), near(keep_up), near(keep_down), near(small))[0]

    turned = [[[(stride * k + start) % owners for k in range(owners)]] for stride, _, start in TURN]
    turned = [None if x[0] == list(range(owners)) else x for x in turned]
    got = lax.all_to_all(send, "kv", 0, 0, axis_index_groups=turned[0], tiled=True)

    stab = saved_stabilizer.transpose(0, 2, 1)
    m0, n0, words, move, bias, first = pl.pallas_call(
        functools.partial(take_kernel, owners=owners, seqs=seqs),
        in_specs=[SMEM] * 4 + [pl.BlockSpec(memory_space=pl.ANY), VMEM],
        out_specs=[VMEM] * 6,
        out_shape=[
            held((own, 1, heads, dim, dim), F32),
            held((own, heads, dim), F32),
            held((heads, own * dim, 2 * dim), BF16),
            held((seqs * props, seqs * props), BF16),
            held((2, per, heads), F32),
            held((own, heads), F32),
        ],
        scratch_shapes=[pltpu.SemaphoreType.DMA((own,))],
        cost_estimate=pl.CostEstimate(flops=40_000_000, bytes_accessed=1_000_000, transcendentals=0),
        name="take",
    )(accepted, stab, input_bias, forget_bias, saved_memory, saved_normalizer)
    steps = props + 1
    gated, kv, coef = pl.pallas_call(
        functools.partial(cell_kernel, features=float(owners * width)),
        in_specs=[VMEM] * 5,
        out_specs=[VMEM] * 3,
        out_shape=[
            held((owners, per, columns), BF16),
            held((2 * heads, per, dim), BF16),
            jax.ShapeDtypeStruct((steps, own, 3 * heads), F32),
        ],
        name="cell",
    )(near(got), near(words), near(n0), near(bias), near(first))

    gathered = lax.all_to_all(gated, "kv", 0, 0, axis_index_groups=turned[1], tiled=True)

    new_memory, new_n, new_s = pl.pallas_call(
        memory_kernel,
        in_specs=[SMEM] + [VMEM] * 3,
        out_specs=[pl.BlockSpec(memory_space=pl.ANY), VMEM, VMEM],
        out_shape=[
            jax.ShapeDtypeStruct((own, steps, heads, dim, dim), F32),
            jax.ShapeDtypeStruct((own, steps, heads, dim), F32),
            jax.ShapeDtypeStruct((own, heads, steps), F32),
        ],
        scratch_shapes=[pltpu.VMEM((own, props, heads, dim, dim), F32), pltpu.SemaphoreType.DMA((own, steps))],
        cost_estimate=pl.CostEstimate(flops=20_000_000, bytes_accessed=3_200_000, transcendentals=0),
        name="memory",
    )(coef, near(m0), near(n0), near(kv))

    terms = pl.pallas_call(
        mix_kernel,
        in_specs=[VMEM] * 2 + [pl.BlockSpec(memory_space=pl.ANY)],
        out_specs=[VMEM],
        out_shape=[held((peers, w_out.shape[1] // peers, seqs * props), BF16)],
        name="mix",
    )(near(gathered), near(w_out), new_s)[0]
    arrived = lax.all_to_all(terms, "tp", split_axis=0, concat_axis=0, tiled=True)

    mixed = pl.pallas_call(
        finish_kernel,
        in_specs=[VMEM] * 2,
        out_specs=VMEM,
        out_shape=jax.ShapeDtypeStruct((props, w_out.shape[1] // peers, seqs), BF16),
        name="finish",
    )(near(arrived), near(move))
    return mixed.transpose(2, 0, 1), new_memory, new_n, new_s.transpose(0, 2, 1)


def solution(mesh):
    return jax.shard_map(
        local,
        mesh=mesh,
        in_specs=(
            P("grp", None, "kv"),
            P(),
            P("kv", "tp"),
            P("kv", "tp"),
            P("kv", "tp"),
            P("kv", "tp"),
            P(),
            P("tp"),
            P("tp"),
            P("tp", "kv"),
            P(("grp", "kv"), None, "tp", None, None),
            P(("grp", "kv"), None, "tp", None),
            P(("grp", "kv"), None, "tp"),
            P(("grp", "kv")),
        ),
        out_specs=(
            P("grp", None, ("kv", "tp")),
            P(("grp", "kv"), None, "tp", None, None),
            P(("grp", "kv"), None, "tp", None),
            P(("grp", "kv"), None, "tp"),
        ),
        check_vma=False,
    )
```

time: 88.7 us -> 84.4 us (0.952)
  waiting for transfers between devices: 19.1 us -> 13.2 us
  starting transfers between devices: 39.4 us -> 44.6 us
  local copies, waits for them, and re-layouts: 3.64 us -> 0.01 us
    all_to_all x2, starting transfers between devices: 16.2 us -> 21.4 us  [the longest x1 17.3 us: local(): lax.all_to_all(gated, 'kv', 0, 0, axis_index_groups=turned[1], tiled=True)]
    gather x2 -> x0, local copies, waits for them, and re-layouts: 3.63 us -> none  [the longest x1 2.32 us: local(): jnp.take_along_axis(saved_memory, accepted[:, None, None, None, None], 1)]
    all_to_all x2, waiting for transfers between devices: 15.8 us -> 12.3 us  [the longest x1 11 us: local(): lax.all_to_all(send, 'kv', 0, 0, axis_index_groups=turned[0], tiled=True)]
    ppermute x1, waiting for transfers between devices: 3.28 us -> 0.85 us  [local(): got_down = lax.ppermute(down, 'kv', with_last)]
    pallas_call x4 -> x6, Pallas kernels: 9.37 us -> 10.9 us  [the longest x1 3.18 us: local(): pl.pallas_call(memory_kernel, in_specs=[SMEM] + [VMEM] * 3, out_specs=[pl...]
  transfers between devices with their start and end apart: 4 -> 4, of which waited for: 3 -> 3; matrix products, arithmetic and copies ran while one was open for 4% -> 0% of each run, Pallas kernels for 6% -> 9%
where the time goes in v4:
time: 84.4 us; the launch traced here: 83.9 us
  starting transfers between devices  44.6 us (53%)
  waiting for transfers between devices  13.2 us (16%)
  blocking collectives  12.8 us (15%)
  Pallas kernels  12.5 us (15%)
    ppermute x1, starting transfers between devices, local(): got_down = lax.ppermute(down, 'kv', with_last)  19.7 us
    all_to_all x1, starting transfers between devices, local(): lax.all_to_all(gated, 'kv', 0, 0, axis_index_groups=turned[1], tiled=True)  17.3 us
    all_to_all x1, blocking collectives, local(): lax.all_to_all(terms, 'tp', split_axis=0, concat_axis=0, tiled=True)  12.8 us
    all_to_all x1, waiting for transfers between devices, local(): lax.all_to_all(send, 'kv', 0, 0, axis_index_groups=turned[0], tiled=True)  11 us
    all_to_all x1, starting transfers between devices, local(): lax.all_to_all(send, 'kv', 0, 0, axis_index_groups=turned[0], tiled=True)  4.15 us
    ppermute x1, starting transfers between devices, local(): got_up = lax.ppermute(up, 'kv', with_next)  3.44 us
    pallas_call x1, Pallas kernels, local(): pl.pallas_call(memory_kernel, in_specs=[SMEM] + [VMEM] * 3, out_specs=[pl...  3.18 us
    pallas_call x1, Pallas kernels, local(): pl.pallas_call(functools.partial(keep_kernel, owners=owners), in_specs=[V...  2.41 us
  transfers between devices with their start and end apart: 4, of which 3 were waited for; matrix products, arithmetic and copies ran while one was open for 0% of the time, Pallas kernels for 9%

profile of v4, /device:TPU:33, one launch (start us, length us, event | category | flops | bytes accessed | tf_op | source)
XLA Modules:
  0.0 83.9 jit_solution(13497703256541376718)
XLA Ops:
  0.6 1.6 %give.1 = (bf16[16,32,128]{2,1,0:T(8,128)(2,1)S(1)}, bf16[16,32,128]{2,1,0:T(8,128)(2,1)S(1)}, bf16[256,256]{1,0:T(8,128)(2,1)S(1)}) custom-call(bf16[64,4,256]{2,1,0:T(4,128)(2,1)} %tokens.3, bf16[32,128]{1,0:T(8,128)(2,1)} %bitcast.7, bf16[256,256]{1,0:T(8,128)(2,1)} %wq.3, bf16[256,256]{1,0:T(8,128)(2,1)} %wk.3, bf16[256,256]{1,0:T(8,128)(2,1)} %wv.3, ...), custom_call_target="tpu_custom_call" | custom-call | tf_op jit(solution)/shard_map/give/pallas_call | solution.py:349
  2.2 3.4 %collective-permute-start = (bf16[16,32,128]{2,1,0:T(8,128)(2,1)S(1)}, bf16[16,32,128]{2,1,0:T(8,128)(2,1)S(1)}, u32[]{:S(2)}, u32[]{:S(2)}) collective-permute-start(bf16[16,32,128]{2,1,0:T(8,128)(2,1)S(1)} %get-tuple-element.22), channel_id=1, source_target_pairs={{0,8},{8,0},{16,24},{24,16},{32,40},{40,32},{48,56},{56,48},{64,72... | collective-permute-start | bytes 393224 | tf_op jit(solution)/shard_map/ppermute | solution.py:363
  5.7 19.7 %collective-permute-start.1 = (bf16[16,32,128]{2,1,0:T(8,128)(2,1)S(1)}, bf16[16,32,128]{2,1,0:T(8,128)(2,1)S(1)}, u32[]{:S(2)}, u32[]{:S(2)}) collective-permute-start(bf16[16,32,128]{2,1,0:T(8,128)(2,1)S(1)} %get-tuple-element.23), channel_id=1, source_target_pairs={{0,120},{8,16},{16,8},{24,32},{32,24},{40,48},{48,40},{56,64},{64,... | collective-permute-start | bytes 393224 | tf_op jit(solution)/shard_map/ppermute | solution.py:364
  25.4 2.4 %keep.1 = (f32[16,32,128]{2,1,0:T(8,128)S(1)}, f32[16,32,128]{2,1,0:T(8,128)S(1)}, bf16[16,8,128]{2,1,0:T(8,128)(2,1)S(1)}) custom-call(bf16[64,4,256]{2,1,0:T(4,128)(2,1)} %tokens.3, bf16[256,256]{1,0:T(8,128)(2,1)S(1)} %get-tuple-element.24.scaled_in, bf16[256,256]{1,0:T(8,128)(2,1)} %wq.3, bf16[256,256]{1,0:T(8,128)(2,1)} %wk.3, bf16[256,256]{1,0:T(8,128)(2,1)} %wv.3, ...), custom_call_target="tpu_custom_call" | custom-call | flops 80000000 | bytes 1000000 | tf_op jit(solution)/shard_map/keep/pallas_call | solution.py:365
  27.8 0.0 collective-permute-done.got_up
  27.8 0.8 %collective-permute-done.1.got_down = bf16[16,32,128]{2,1,0:T(8,128)(2,1)S(1)} collective-permute-done((bf16[16,32,128]{2,1,0:T(8,128)(2,1)S(1)}, bf16[16,32,128]{2,1,0:T(8,128)(2,1)S(1)}, u32[]{:S(2)}, u32[]{:S(2)}) %collective-permute-start.1) | collective-permute-done | bytes 131104 | tf_op jit(solution)/shard_map/ppermute | solution.py:364
  28.7 0.9 %merge.1 = bf16[16,72,128]{2,1,0:T(8,128)(2,1)} custom-call(bf16[16,32,128]{2,1,0:T(8,128)(2,1)S(1)} %collective-permute-done.got_up, bf16[16,32,128]{2,1,0:T(8,128)(2,1)S(1)} %collective-permute-done.1.got_down, f32[16,32,128]{2,1,0:T(8,128)S(1)} %get-tuple-element.25.keep_up, f32[16,32,128]{2,1,0:T(8,128)S(1)} %get-tuple-element.26.keep_down, ...), custom_call_target="tpu_custom_call" | custom-call | tf_op jit(solution)/shard_map/merge/pallas_call | solution.py:378
  29.6 0.0 copy-start
  29.7 4.1 %all-to-all-start = ((bf16[16,72,128]{2,1,0:T(8,128)(2,1)}), bf16[16,72,128]{2,1,0:T(8,128)(2,1)S(1)}, u32[]{:S(2)}, u32[]{:S(2)}) async-start(bf16[16,72,128]{2,1,0:T(8,128)(2,1)} %merge.1), calls=%async_computation | async-start | bytes 589824 | tf_op jit(solution)/shard_map/all_to_all | solution.py:389
  33.8 1.9 %take.1 = (f32[4,1,2,128,128]{4,3,2,1,0:T(8,128)S(1)}, f32[4,2,128]{2,1,0:T(2,128)S(1)}, bf16[2,512,256]{2,1,0:T(8,128)(2,1)S(1)}, bf16[256,256]{1,0:T(8,128)(2,...) custom-call(s32[4]{0:T(128)} %accepted.1, f32[4,2,5]{2,1,0:T(2,128)} %bitcast.8, f32[2]{0:T(128)} %ib.1, f32[2]{0:T(128)} %fb.1, ...), custom_call_target="tpu_custom_call" | custom-call | flops 40000000 | bytes 1000000 | tf_op jit(solution)/shard_map/take/pallas_call | solution.py:392
  35.7 11.0 %all-to-all-done.got = bf16[16,72,128]{2,1,0:T(8,128)(2,1)S(1)} async-done(((bf16[16,72,128]{2,1,0:T(8,128)(2,1)}), bf16[16,72,128]{2,1,0:T(8,128)(2,1)S(1)}, u32[]{:S(2)}, u32[]{:S(2)}) %all-to-all-start) | async-done | bytes 294944 | tf_op jit(solution)/shard_map/all_to_all | solution.py:389
  46.7 1.4 %cell.1 = (bf16[16,16,256]{2,1,0:T(8,128)(2,1)}, bf16[4,16,128]{2,1,0:T(8,128)(2,1)S(1)}, f32[5,4,6]{2,1,0:T(4,128)}) custom-call(bf16[16,72,128]{2,1,0:T(8,128)(2,1)S(1)} %all-to-all-done.got, bf16[2,512,256]{2,1,0:T(8,128)(2,1)S(1)} %get-tuple-element.28.words, f32[4,2,128]{2,1,0:T(2,128)S(1)} %get-tuple-element.29.n0, ...), custom_call_target="tpu_custom_call" | custom-call | tf_op jit(solution)/shard_map/cell/pallas_call | solution.py:409
  48.1 17.3 %all-to-all-start.1 = ((bf16[16,16,256]{2,1,0:T(8,128)(2,1)}), bf16[16,16,256]{2,1,0:T(8,128)(2,1)S(1)}, u32[]{:S(2)}, u32[]{:S(2)}) async-start(bf16[16,16,256]{2,1,0:T(8,128)(2,1)} %get-tuple-element.32), calls=%async_computation.1 | async-start | bytes 262144 | tf_op jit(solution)/shard_map/all_to_all | solution.py:421
  65.4 3.2 %memory.1 = (f32[4,5,2,128,128]{4,3,2,1,0:T(8,128)}, f32[4,5,2,128]{3,2,1,0:T(2,128)}, f32[4,2,5]{2,1,0:T(2,128)}) custom-call(f32[5,4,6]{2,1,0:T(4,128)} %get-tuple-element.33.coef, f32[4,1,2,128,128]{4,3,2,1,0:T(8,128)S(1)} %get-tuple-element.34.m0, f32[4,2,128]{2,1,0:T(2,128)S(1)} %get-tuple-element.29.n0, bf16[4,16,128]{2,1,0:T(8,128)(2,1)S(1)} %get-tuple-element.35.kv), custom_call_target="tpu_custom_call" | custom-call | flops 20000000 | bytes 3200000 | tf_op jit(solution)/shard_map/memory/pallas_call | solution.py:423
  68.6 1.4 %all-to-all-done.1.gathered = bf16[16,16,256]{2,1,0:T(8,128)(2,1)S(1)} async-done(((bf16[16,16,256]{2,1,0:T(8,128)(2,1)}), bf16[16,16,256]{2,1,0:T(8,128)(2,1)S(1)}, u32[]{:S(2)}, u32[]{:S(2)}) %all-to-all-start.1) | async-done | bytes 131104 | tf_op jit(solution)/shard_map/all_to_all | solution.py:421
  70.0 0.0 copy-done
  70.0 0.2 mix.1
  70.2 12.8 %all_to_all.15.got = bf16[8,32,256]{2,1,0:T(8,128)(2,1)S(1)} all-to-all(bf16[8,32,256]{2,1,0:T(8,128)(2,1)S(1)} %mix.1), channel_id=1, replica_groups=mesh['grp'=2,'kv'=16,'tp'=8] {'tp'}, dimensions={0} | all-to-all | bytes 262144 | tf_op jit(solution)/shard_map/all_to_all | solution.py:444
  83.0 0.8 finish.1
Async XLA Ops:
  2.2 25.6 %collective-permute-start = (bf16[16,32,128]{2,1,0:T(8,128)(2,1)S(1)}, bf16[16,32,128]{2,1,0:T(8,128)(2,1)S(1)}, u32[]{:S(2)}, u32[]{:S(2)}) collective-permute-start(bf16[16,32,128]{2,1,0:T(8,128)(2,1)S(1)} %get-tuple-element.22), channel_id=1, source_target_pairs={{0,8},{8,0},{16,24},{24,16},{32,40},{40,32},{48,56},{56,48},{64,72... | collective-permute-start | bytes 393224 | tf_op jit(solution)/shard_map/ppermute | solution.py:363
  5.7 23.0 %collective-permute-start.1 = (bf16[16,32,128]{2,1,0:T(8,128)(2,1)S(1)}, bf16[16,32,128]{2,1,0:T(8,128)(2,1)S(1)}, u32[]{:S(2)}, u32[]{:S(2)}) collective-permute-start(bf16[16,32,128]{2,1,0:T(8,128)(2,1)S(1)} %get-tuple-element.23), channel_id=1, source_target_pairs={{0,120},{8,16},{16,8},{24,32},{32,24},{40,48},{48,40},{56,64},{64,... | collective-permute-start | bytes 393224 | tf_op jit(solution)/shard_map/ppermute | solution.py:364
  29.6 40.3 %copy-start = (bf16[256,256]{1,0:T(8,128)(2,1)S(1)}, bf16[256,256]{1,0:T(8,128)(2,1)}, u32[]{:S(2)}) copy-start(bf16[256,256]{1,0:T(8,128)(2,1)} %w.1) | copy-start | bytes 393220
  29.7 17.0 %all-to-all-start = ((bf16[16,72,128]{2,1,0:T(8,128)(2,1)}), bf16[16,72,128]{2,1,0:T(8,128)(2,1)S(1)}, u32[]{:S(2)}, u32[]{:S(2)}) async-start(bf16[16,72,128]{2,1,0:T(8,128)(2,1)} %merge.1), calls=%async_computation | async-start | bytes 589824 | tf_op jit(solution)/shard_map/all_to_all | solution.py:389
  48.1 21.8 %all-to-all-start.1 = ((bf16[16,16,256]{2,1,0:T(8,128)(2,1)}), bf16[16,16,256]{2,1,0:T(8,128)(2,1)S(1)}, u32[]{:S(2)}, u32[]{:S(2)}) async-start(bf16[16,16,256]{2,1,0:T(8,128)(2,1)} %get-tuple-element.32), calls=%async_computation.1 | async-start | bytes 262144 | tf_op jit(solution)/shard_map/all_to_all | solution.py:421

commit v5 on v4

--- a/solution.py
+++ b/solution.py
@@ -45,9 +45,16 @@
     return [y[:, h * 128 : (h + 1) * 128].reshape(owners, -1, 128) for h in range(y.shape[1] // 128)]
 
 
-def give_kernel(tokens, gain, wq, wk, wv, wo, up, down, scaled_out, *, owners):
+def give_kernel(tokens, gain, wq, wk, wv, wo, up, down, scaled_out, theirs, sems, *, owners):
     z = lax.axis_index("kv")
     seqs, props, width = tokens.shape
+    even = (z & 1) == 0
+    copies = []
+    for k, (first, second) in enumerate(((wq, wk), (wv, wo))):
+        copies.append(pltpu.make_async_copy(second, theirs.at[k], sems.at[k]))
+        other = pltpu.make_async_copy(first, theirs.at[k], sems.at[k])
+        pl.when(even)(copies[k].start)
+        pl.when(jnp.logical_not(even))(other.start)
     rows = seqs * props
     per = rows // owners
     own = per // props
@@ -60,10 +67,9 @@
     scaled = (x * jnp.concatenate(pieces, 1)).astype(BF16)
     scaled = contract(moved_rows(rows, per, own), scaled, 1, 0).astype(BF16)
     scaled_out[...] = scaled
-    even = (z & 1) == 0
-    for first, second, given in ((wq, wk, up), (wv, wo, down)):
-        theirs = jnp.where(even, second[...], first[...])
-        for h, y in enumerate(blocked(coded(contract(scaled, theirs, 1, 0)), owners)):
+    for k, given in enumerate((up, down)):
+        copies[k].wait()
+        for h, y in enumerate(blocked(coded(contract(scaled, theirs[k], 1, 0)), owners)):
             given[:, h * per : (h + 1) * per, :] = y
 
 
@@ -348,13 +354,14 @@
     weights = (w_query, w_key, w_value, w_outgate)
     up, down, scaled = pl.pallas_call(
         functools.partial(give_kernel, owners=owners),
-        in_specs=[VMEM] * 6,
+        in_specs=[VMEM] * 2 + [pl.BlockSpec(memory_space=pl.ANY)] * 4,
         out_specs=[VMEM] * 3,
         out_shape=[
             held((owners, half, 128), BF16),
             held((owners, half, 128), BF16),
             held((seqs * props, width), BF16),
         ],
+        scratch_shapes=[pltpu.VMEM((2, *w_query.shape), BF16), pltpu.SemaphoreType.DMA((2,))],
         name="give",
     )(tokens, norm_gain.reshape(-1, 128), *weights)
 

time: 84.4 us -> 85.1 us (level)
  no operation moved by 1% of the time
where the time goes in v5:
time: 85.1 us; the launch traced here: 84.6 us
  starting transfers between devices  44.6 us (52%)
  Pallas kernels  13.2 us (16%)
  waiting for transfers between devices  13.2 us (16%)
  blocking collectives  12.9 us (15%)
    ppermute x1, starting transfers between devices, local(): got_down = lax.ppermute(down, 'kv', with_last)  19.8 us
    all_to_all x1, starting transfers between devices, local(): lax.all_to_all(gated, 'kv', 0, 0, axis_index_groups=turned[1], tiled=True)  17.3 us
    all_to_all x1, blocking collectives, local(): lax.all_to_all(terms, 'tp', split_axis=0, concat_axis=0, tiled=True)  12.9 us
    all_to_all x1, waiting for transfers between devices, local(): lax.all_to_all(send, 'kv', 0, 0, axis_index_groups=turned[0], tiled=True)  11 us
    all_to_all x1, starting transfers between devices, local(): lax.all_to_all(send, 'kv', 0, 0, axis_index_groups=turned[0], tiled=True)  4.14 us
    ppermute x1, starting transfers between devices, local(): got_up = lax.ppermute(up, 'kv', with_next)  3.43 us
    pallas_call x1, Pallas kernels, local(): pl.pallas_call(memory_kernel, in_specs=[SMEM] + [VMEM] * 3, out_specs=[pl...  3.18 us
    pallas_call x1, Pallas kernels, local(): pl.pallas_call(functools.partial(keep_kernel, owners=owners), in_specs=[V...  2.41 us
  transfers between devices with their start and end apart: 4, of which 3 were waited for; matrix products, arithmetic and copies ran while one was open for 0% of the time, Pallas kernels for 9%

profile of v5, /device:TPU:33, one launch (start us, length us, event | category | flops | bytes accessed | tf_op | source)
XLA Modules:
  0.0 84.6 jit_solution(5936104134761930695)
XLA Ops:
  0.6 2.3 %give.1 = (bf16[16,32,128]{2,1,0:T(8,128)(2,1)S(1)}, bf16[16,32,128]{2,1,0:T(8,128)(2,1)S(1)}, bf16[256,256]{1,0:T(8,128)(2,1)S(1)}) custom-call(bf16[64,4,256]{2,1,0:T(4,128)(2,1)} %tokens.3, bf16[32,128]{1,0:T(8,128)(2,1)} %bitcast.7, bf16[256,256]{1,0:T(8,128)(2,1)} %wq.3, bf16[256,256]{1,0:T(8,128)(2,1)} %wk.3, bf16[256,256]{1,0:T(8,128)(2,1)} %wv.3, ...), custom_call_target="tpu_custom_call" | custom-call | tf_op jit(solution)/shard_map/give/pallas_call | solution.py:355
  2.9 3.4 %collective-permute-start = (bf16[16,32,128]{2,1,0:T(8,128)(2,1)S(1)}, bf16[16,32,128]{2,1,0:T(8,128)(2,1)S(1)}, u32[]{:S(2)}, u32[]{:S(2)}) collective-permute-start(bf16[16,32,128]{2,1,0:T(8,128)(2,1)S(1)} %get-tuple-element.22), channel_id=1, source_target_pairs={{0,8},{8,0},{16,24},{24,16},{32,40},{40,32},{48,56},{56,48},{64,72... | collective-permute-start | bytes 393224 | tf_op jit(solution)/shard_map/ppermute | solution.py:370
  6.4 19.8 %collective-permute-start.1 = (bf16[16,32,128]{2,1,0:T(8,128)(2,1)S(1)}, bf16[16,32,128]{2,1,0:T(8,128)(2,1)S(1)}, u32[]{:S(2)}, u32[]{:S(2)}) collective-permute-start(bf16[16,32,128]{2,1,0:T(8,128)(2,1)S(1)} %get-tuple-element.23), channel_id=1, source_target_pairs={{0,120},{8,16},{16,8},{24,32},{32,24},{40,48},{48,40},{56,64},{64,... | collective-permute-start | bytes 393224 | tf_op jit(solution)/shard_map/ppermute | solution.py:371
  26.1 2.4 %keep.1 = (f32[16,32,128]{2,1,0:T(8,128)S(1)}, f32[16,32,128]{2,1,0:T(8,128)S(1)}, bf16[16,8,128]{2,1,0:T(8,128)(2,1)S(1)}) custom-call(bf16[64,4,256]{2,1,0:T(4,128)(2,1)} %tokens.3, bf16[256,256]{1,0:T(8,128)(2,1)S(1)} %get-tuple-element.24.scaled_in, bf16[256,256]{1,0:T(8,128)(2,1)} %wq.3, bf16[256,256]{1,0:T(8,128)(2,1)} %wk.3, bf16[256,256]{1,0:T(8,128)(2,1)} %wv.3, ...), custom_call_target="tpu_custom_call" | custom-call | flops 80000000 | bytes 1000000 | tf_op jit(solution)/shard_map/keep/pallas_call | solution.py:372
  28.5 0.0 collective-permute-done.got_up
  28.5 0.8 %collective-permute-done.1.got_down = bf16[16,32,128]{2,1,0:T(8,128)(2,1)S(1)} collective-permute-done((bf16[16,32,128]{2,1,0:T(8,128)(2,1)S(1)}, bf16[16,32,128]{2,1,0:T(8,128)(2,1)S(1)}, u32[]{:S(2)}, u32[]{:S(2)}) %collective-permute-start.1) | collective-permute-done | bytes 131104 | tf_op jit(solution)/shard_map/ppermute | solution.py:371
  29.4 0.9 %merge.1 = bf16[16,72,128]{2,1,0:T(8,128)(2,1)} custom-call(bf16[16,32,128]{2,1,0:T(8,128)(2,1)S(1)} %collective-permute-done.got_up, bf16[16,32,128]{2,1,0:T(8,128)(2,1)S(1)} %collective-permute-done.1.got_down, f32[16,32,128]{2,1,0:T(8,128)S(1)} %get-tuple-element.25.keep_up, f32[16,32,128]{2,1,0:T(8,128)S(1)} %get-tuple-element.26.keep_down, ...), custom_call_target="tpu_custom_call" | custom-call | tf_op jit(solution)/shard_map/merge/pallas_call | solution.py:385
  30.3 0.0 copy-start
  30.4 4.1 %all-to-all-start = ((bf16[16,72,128]{2,1,0:T(8,128)(2,1)}), bf16[16,72,128]{2,1,0:T(8,128)(2,1)S(1)}, u32[]{:S(2)}, u32[]{:S(2)}) async-start(bf16[16,72,128]{2,1,0:T(8,128)(2,1)} %merge.1), calls=%async_computation | async-start | bytes 589824 | tf_op jit(solution)/shard_map/all_to_all | solution.py:396
  34.5 1.9 %take.1 = (f32[4,1,2,128,128]{4,3,2,1,0:T(8,128)S(1)}, f32[4,2,128]{2,1,0:T(2,128)S(1)}, bf16[2,512,256]{2,1,0:T(8,128)(2,1)S(1)}, bf16[256,256]{1,0:T(8,128)(2,...) custom-call(s32[4]{0:T(128)} %accepted.1, f32[4,2,5]{2,1,0:T(2,128)} %bitcast.8, f32[2]{0:T(128)} %ib.1, f32[2]{0:T(128)} %fb.1, ...), custom_call_target="tpu_custom_call" | custom-call | flops 40000000 | bytes 1000000 | tf_op jit(solution)/shard_map/take/pallas_call | solution.py:399
  36.4 11.0 %all-to-all-done.got = bf16[16,72,128]{2,1,0:T(8,128)(2,1)S(1)} async-done(((bf16[16,72,128]{2,1,0:T(8,128)(2,1)}), bf16[16,72,128]{2,1,0:T(8,128)(2,1)S(1)}, u32[]{:S(2)}, u32[]{:S(2)}) %all-to-all-start) | async-done | bytes 294944 | tf_op jit(solution)/shard_map/all_to_all | solution.py:396
  47.4 1.4 %cell.1 = (bf16[16,16,256]{2,1,0:T(8,128)(2,1)}, bf16[4,16,128]{2,1,0:T(8,128)(2,1)S(1)}, f32[5,4,6]{2,1,0:T(4,128)}) custom-call(bf16[16,72,128]{2,1,0:T(8,128)(2,1)S(1)} %all-to-all-done.got, bf16[2,512,256]{2,1,0:T(8,128)(2,1)S(1)} %get-tuple-element.28.words, f32[4,2,128]{2,1,0:T(2,128)S(1)} %get-tuple-element.29.n0, ...), custom_call_target="tpu_custom_call" | custom-call | tf_op jit(solution)/shard_map/cell/pallas_call | solution.py:416
  48.8 17.3 %all-to-all-start.1 = ((bf16[16,16,256]{2,1,0:T(8,128)(2,1)}), bf16[16,16,256]{2,1,0:T(8,128)(2,1)S(1)}, u32[]{:S(2)}, u32[]{:S(2)}) async-start(bf16[16,16,256]{2,1,0:T(8,128)(2,1)} %get-tuple-element.32), calls=%async_computation.1 | async-start | bytes 262144 | tf_op jit(solution)/shard_map/all_to_all | solution.py:428
  66.1 3.2 %memory.1 = (f32[4,5,2,128,128]{4,3,2,1,0:T(8,128)}, f32[4,5,2,128]{3,2,1,0:T(2,128)}, f32[4,2,5]{2,1,0:T(2,128)}) custom-call(f32[5,4,6]{2,1,0:T(4,128)} %get-tuple-element.33.coef, f32[4,1,2,128,128]{4,3,2,1,0:T(8,128)S(1)} %get-tuple-element.34.m0, f32[4,2,128]{2,1,0:T(2,128)S(1)} %get-tuple-element.29.n0, bf16[4,16,128]{2,1,0:T(8,128)(2,1)S(1)} %get-tuple-element.35.kv), custom_call_target="tpu_custom_call" | custom-call | flops 20000000 | bytes 3200000 | tf_op jit(solution)/shard_map/memory/pallas_call | solution.py:430
  69.3 1.4 %all-to-all-done.1.gathered = bf16[16,16,256]{2,1,0:T(8,128)(2,1)S(1)} async-done(((bf16[16,16,256]{2,1,0:T(8,128)(2,1)}), bf16[16,16,256]{2,1,0:T(8,128)(2,1)S(1)}, u32[]{:S(2)}, u32[]{:S(2)}) %all-to-all-start.1) | async-done | bytes 131104 | tf_op jit(solution)/shard_map/all_to_all | solution.py:428
  70.6 0.0 copy-done
  70.6 0.2 mix.1
  70.9 12.9 %all_to_all.15.got = bf16[8,32,256]{2,1,0:T(8,128)(2,1)S(1)} all-to-all(bf16[8,32,256]{2,1,0:T(8,128)(2,1)S(1)} %mix.1), channel_id=1, replica_groups=mesh['grp'=2,'kv'=16,'tp'=8] {'tp'}, dimensions={0} | all-to-all | bytes 262144 | tf_op jit(solution)/shard_map/all_to_all | solution.py:451
  83.7 0.8 finish.1
Async XLA Ops:
  2.9 25.6 %collective-permute-start = (bf16[16,32,128]{2,1,0:T(8,128)(2,1)S(1)}, bf16[16,32,128]{2,1,0:T(8,128)(2,1)S(1)}, u32[]{:S(2)}, u32[]{:S(2)}) collective-permute-start(bf16[16,32,128]{2,1,0:T(8,128)(2,1)S(1)} %get-tuple-element.22), channel_id=1, source_target_pairs={{0,8},{8,0},{16,24},{24,16},{32,40},{40,32},{48,56},{56,48},{64,72... | collective-permute-start | bytes 393224 | tf_op jit(solution)/shard_map/ppermute | solution.py:370
  6.4 23.0 %collective-permute-start.1 = (bf16[16,32,128]{2,1,0:T(8,128)(2,1)S(1)}, bf16[16,32,128]{2,1,0:T(8,128)(2,1)S(1)}, u32[]{:S(2)}, u32[]{:S(2)}) collective-permute-start(bf16[16,32,128]{2,1,0:T(8,128)(2,1)S(1)} %get-tuple-element.23), channel_id=1, source_target_pairs={{0,120},{8,16},{16,8},{24,32},{32,24},{40,48},{48,40},{56,64},{64,... | collective-permute-start | bytes 393224 | tf_op jit(solution)/shard_map/ppermute | solution.py:371
  30.3 40.3 %copy-start = (bf16[256,256]{1,0:T(8,128)(2,1)S(1)}, bf16[256,256]{1,0:T(8,128)(2,1)}, u32[]{:S(2)}) copy-start(bf16[256,256]{1,0:T(8,128)(2,1)} %w.1) | copy-start | bytes 393220
  30.4 17.0 %all-to-all-start = ((bf16[16,72,128]{2,1,0:T(8,128)(2,1)}), bf16[16,72,128]{2,1,0:T(8,128)(2,1)S(1)}, u32[]{:S(2)}, u32[]{:S(2)}) async-start(bf16[16,72,128]{2,1,0:T(8,128)(2,1)} %merge.1), calls=%async_computation | async-start | bytes 589824 | tf_op jit(solution)/shard_map/all_to_all | solution.py:396
  48.8 21.8 %all-to-all-start.1 = ((bf16[16,16,256]{2,1,0:T(8,128)(2,1)}), bf16[16,16,256]{2,1,0:T(8,128)(2,1)S(1)}, u32[]{:S(2)}, u32[]{:S(2)}) async-start(bf16[16,16,256]{2,1,0:T(8,128)(2,1)} %get-tuple-element.32), calls=%async_computation.1 | async-start | bytes 262144 | tf_op jit(solution)/shard_map/all_to_all | solution.py:428
